TPU v7x, 128 devices: a whole 4x4x4 slice. The times are simulated.
128 devices in a mesh: tp: 16 (over z, y), dp: 8 (over x, core).
Axes of the slice: x: 4, y: 4, z: 4, core: 2. Of those that a mesh axis runs over, the one named last changes fastest.
Arguments:
- tokens: bfloat16 [256, 4096], P('tp', 'dp'), may hold values from -10 to 10
- norm_gain: float32 [2, 4096], P(None, 'dp'), may hold values from 0.1 to 1.9
- input_weight: bfloat16 [2, 4096, 1024], P(None, 'dp', 'tp'), may hold values from -0.09375 to 0.09375
- decay_rate: float32 [2, 64, 64], P(None, 'tp'), may hold values from 0.01 to 1
- frequency: float32 [2, 64, 64], P(None, 'tp'), may hold values from 0.5 to 3
- step_size: float32 [2, 64], P(None, 'tp'), may hold values from 0.1 to 1
- state_in: float32 [2, 64, 16, 128], P(None, 'tp'), may hold values from -1.5 to 1.5
- readout: float32 [2, 64, 16, 128], P(None, 'tp'), may hold values from -0.5 to 0.5
- skip_gain: float32 [2, 1024], P(None, 'tp'), may hold values from -3 to 3
- value_weight: bfloat16 [2, 1024, 4096], P(None, 'tp', 'dp'), may hold values from -0.1875 to 0.1875
- gate_weight: bfloat16 [2, 1024, 4096], P(None, 'tp', 'dp'), may hold values from -0.1875 to 0.1875
- states: float32 [2, 256, 64, 128], P(None, 'dp', 'tp'), may hold values from -3 to 3
Outputs:
- tokens_out: bfloat16 [256, 4096], P('tp', 'dp')
- states_out: float32 [2, 256, 64, 128], P(None, 'dp', 'tp')
All inputs are finite; a program needn't handle non-finite values.
Results may differ from a plain program's by a relative error of at most 0.007.
Values may be sent and summed in bfloat16 or wider, within the bound.
A program may use at most 64 MiB of HBM per device.

v0:
```python
import jax
import jax.numpy as jnp
from jax import lax
from jax.sharding import PartitionSpec as P

D = 4096
LAYERS = 2


epsilon = 1e-06


def copy_for_each(shard, axis):
    devices = lax.axis_size(axis)
    return lax.all_to_all(
        jnp.broadcast_to(shard[None], (devices, *shard.shape)), axis, 0, 0, tiled=True
    )


def joined_along(tiles, dim):
    tiles = jnp.moveaxis(tiles, 0, dim)
    shape = tiles.shape
    return tiles.reshape(*shape[:dim], shape[dim] * shape[dim + 1], *shape[dim + 2 :])


def gathered_copies(shard, axis, dim):
    tiles = copy_for_each(shard, axis)
    return joined_along(tiles, dim)


def split_up(shard, dim, devices):
    shape = shard.shape
    tiles = shard.reshape(*shape[:dim], devices, shape[dim] // devices, *shape[dim + 1 :])
    return jnp.moveaxis(tiles, dim, 0)


def sent_and_summed(shard, axis, dim):
    devices = lax.axis_size(axis)
    tiles = lax.all_to_all(split_up(shard, dim, devices), axis, 0, 0, tiled=True)
    return jnp.sum(tiles, axis=0)


def in_one_piece(arrays, axis, dim, along):
    columns = [a.reshape(*a.shape[:along], -1) for a in arrays]
    both = jnp.concatenate(columns, axis=along)
    filled, at, outs = (sent_and_summed(both, axis, dim), 0, [])
    for a, column in zip(arrays, columns):
        piece = filled[..., at : at + column.shape[along]]
        outs.append(piece.reshape(*piece.shape[:along], *a.shape[along:]))
        at += column.shape[along]
    return tuple(outs)


def sent_together(arrays, axis, dim, along):
    ends, at = ([], 0)
    for a in arrays[:-1]:
        at += a.shape[along]
        ends.append(at)
    both = jnp.concatenate(arrays, axis=along)
    return tuple(jnp.split(lax.all_gather(both, axis, axis=dim, tiled=True), ends, axis=along))


def transition(rate, frequency, step):
    magnitude = jnp.exp(-rate * step[:, None])
    angle = frequency * step[:, None]
    keep_real = magnitude * jnp.cos(angle)
    keep_imag = magnitude * jnp.sin(angle)
    minus_one = keep_real - 1.0
    denominator = rate * rate + frequency * frequency
    lift_real = (-minus_one * rate + keep_imag * frequency) / denominator
    lift_imag = (-keep_imag * rate - minus_one * frequency) / denominator
    return (keep_real, keep_imag, lift_real, lift_imag)


def update(drive, state, rate, frequency, step, state_in, readout, skip):
    groups = rate.shape[0]
    half = state.shape[-1] // 2
    grouped = drive.reshape(drive.shape[0], groups, -1)
    pushed = jnp.einsum("sgc,gcq->sgq", grouped, state_in)
    keep_real, keep_imag, lift_real, lift_imag = transition(rate, frequency, step)
    push_real, push_imag = (pushed[..., :half], pushed[..., half:])
    old_real, old_imag = (state[..., :half], state[..., half:])
    new_real = (
        keep_real * old_real - keep_imag * old_imag + lift_real * push_real - lift_imag * push_imag
    )
    new_imag = (
        keep_real * old_imag + keep_imag * old_real + lift_real * push_imag + lift_imag * push_real
    )
    new_state = jnp.concatenate([new_real, new_imag], axis=-1)
    summed = jnp.einsum("sgq,gcq->sgc", new_state, readout)
    value = summed.reshape(drive.shape) + skip[None, :] * drive
    return (new_state, jax.nn.gelu(value).astype(jnp.bfloat16))


def body(
    tokens,
    norm_gain,
    input_weight,
    decay_rate,
    frequency,
    step_size,
    state_in,
    readout,
    skip_gain,
    value_weight,
    gate_weight,
    states,
):
    current = tokens
    updated = []
    for depth_index in range(LAYERS):
        whole = gathered_copies(current, "tp", 0)
        widened = whole.astype(jnp.float32)
        squares = jnp.sum(widened * widened, axis=1)
        gained = (widened * norm_gain[depth_index][None, :]).astype(jnp.bfloat16)
        weight_in = input_weight[depth_index]
        partial_terms = jnp.dot(gained, weight_in, preferred_element_type=jnp.float32)
        summed, own_squares = in_one_piece((partial_terms, squares), "dp", 0, 1)
        drive = summed * lax.rsqrt(own_squares / D + epsilon)[:, None]
        new_state, readout_value = update(
            drive,
            states[depth_index],
            decay_rate[depth_index],
            frequency[depth_index],
            step_size[depth_index],
            state_in[depth_index],
            readout[depth_index],
            skip_gain[depth_index],
        )
        updated.append(new_state)
        ready = gathered_copies(readout_value, "dp", 0)
        value_rows = value_weight[depth_index]
        gate_rows = gate_weight[depth_index]
        mixed = lax.all_to_all(ready, "tp", split_axis=0, concat_axis=1, tiled=True)
        pieces = sent_together((value_rows, gate_rows), "tp", 0, 1)
        value = jnp.dot(mixed, pieces[0], preferred_element_type=jnp.float32)
        gate = jnp.dot(mixed, pieces[1], preferred_element_type=jnp.float32)
        current = (current.astype(jnp.float32) + value * jax.nn.sigmoid(gate)).astype(jnp.bfloat16)
    return (current, jnp.stack(updated))


def solution(mesh):
    in_specs = (
        P("tp", "dp"),
        P(None, "dp"),
        P(None, "dp", "tp"),
        P(None, "tp", None),
        P(None, "tp", None),
        P(None, "tp"),
        P(None, "tp", None, None),
        P(None, "tp", None, None),
        P(None, "tp"),
        P(None, "tp", "dp"),
        P(None, "tp", "dp"),
        P(None, "dp", "tp", None),
    )
    out_specs = (P("tp", "dp"), P(None, "dp", "tp", None))
    return jax.shard_map(body, mesh=mesh, in_specs=in_specs, out_specs=out_specs, check_vma=False)
```

profile of v0, /device:TPU:1, one launch (start us, length us, event | category | flops | bytes accessed | tf_op | source)
XLA Modules:
  0.0 118.7 jit_solution(6991798554835711015)
XLA Ops:
  7.3 1.0 slice_bitcast_fusion
  8.3 0.7 pad_maximum_fusion.1
  9.0 1.5 %broadcast_in_dim.8 = bf16[16,16,512]{2,1,0:T(8,128)(2,1)} broadcast(bf16[16,512]{1,0:T(8,128)(2,1)} %param.12), dimensions={1,2} | broadcast | bytes 278528 | tf_op jit(solution)/shard_map/broadcast_in_dim | solution.py:16
  10.5 8.7 %all-to-all-start = ((bf16[16,16,512]{2,1,0:T(8,128)(2,1)}), bf16[16,16,512]{2,1,0:T(8,128)(2,1)S(1)}, u32[]{:S(2)}, u32[]{:S(2)}) async-start(bf16[16,16,512]{2,1,0:T(8,128)(2,1)} %broadcast_in_dim.8), calls=%async_computation | async-start | bytes 524288 | tf_op jit(solution)/shard_map/all_to_all | solution.py:15
  19.3 0.6 pad_maximum_fusion.3
  20.1 0.1 fusion.66
  20.2 0.1 fusion.64
  20.4 6.4 %all-to-all-done = bf16[16,16,512]{2,1,0:T(8,128)(2,1)S(1)} async-done(((bf16[16,16,512]{2,1,0:T(8,128)(2,1)}), bf16[16,16,512]{2,1,0:T(8,128)(2,1)S(1)}, u32[]{:S(2)}, u32[]{:S(2)}) %all-to-all-start) | async-done | bytes 262176 | tf_op jit(solution)/shard_map/all_to_all | solution.py:15
  26.8 0.2 fusion.18
  27.1 0.2 fusion.24
  27.3 0.8 pad_maximum_fusion
  28.0 6.4 %all-to-all-start.1 = ((f32[8,32,65]{2,1,0:T(8,128)}), f32[8,32,65]{2,1,0:T(8,128)S(1)}, u32[]{:S(2)}, u32[]{:S(2)}) async-start(f32[8,32,65]{2,1,0:T(8,128)} %pad_maximum_fusion), calls=%async_computation.1 | async-start | bytes 262144 | tf_op jit(solution)/shard_map/all_to_all | solution.py:39
  34.4 5.2 %all-to-all-done.1 = f32[8,32,65]{2,1,0:T(8,128)S(1)} async-done(((f32[8,32,65]{2,1,0:T(8,128)}), f32[8,32,65]{2,1,0:T(8,128)S(1)}, u32[]{:S(2)}, u32[]{:S(2)}) %all-to-all-start.1) | async-done | bytes 66592 | tf_op jit(solution)/shard_map/all_to_all | solution.py:39
  39.7 0.2 fusion.61
  40.1 0.2 convolution_bitcast_fusion.1
  40.3 0.1 multiply_subtract_fusion.1
  40.4 0.2 fusion.31
  40.8 0.1 reshape.170
  40.9 8.0 %all_to_all.68 = bf16[8,2,1024]{2,1,0:T(2,128)(2,1)S(1)} all-to-all(bf16[8,2,1024]{2,1,0:T(2,128)(2,1)S(1)} %reshape.170), channel_id=1, replica_groups=mesh['tp'=16,'dp'=8] {'dp'}, dimensions={0} | all-to-all | bytes 65536 | tf_op jit(solution)/shard_map/all_to_all | solution.py:15
  48.9 0.1 reshape.171
  49.0 0.1 reshape.172
  49.1 9.1 %all_to_all.69 = bf16[16,2,512]{2,1,0:T(2,128)(2,1)S(1)} all-to-all(bf16[16,2,512]{2,1,0:T(2,128)(2,1)S(1)} %reshape.172), channel_id=1, replica_groups=mesh['tp'=16,'dp'=8] {'tp'}, dimensions={0} | all-to-all | bytes 65536 | tf_op jit(solution)/shard_map/all_to_all | solution.py:134
  58.2 0.1 reshape.173
  58.4 0.1 all_to_all.52
  58.5 1.5 %fusion.16 = f32[16,512]{1,0:T(8,128)S(1)} fusion(bf16[16,1024]{1,0:T(8,128)(2,1)S(1)} %all_to_all.52, bf16[1024,1024]{1,0:T(8,128)(2,1)} %all-gather.3.cloned.1.call-done), kind=kOutput, calls=%fused_computation.20 | convolution fusion | flops 16777216 | bytes 1114112 | tf_op jit(solution)/shard_map/dot_general | solution.py:136
  60.0 1.5 %fusion.10 = bf16[16,512]{1,0:T(8,128)(2,1)S(1)} fusion(f32[16,512]{1,0:T(8,128)S(1)} %fusion.16, bf16[16,1024]{1,0:T(8,128)(2,1)S(1)} %all_to_all.52, bf16[1024,1024]{1,0:T(8,128)(2,1)} %all-gather.3.cloned.1.call-done, bf16[16,512]{1,0:T(8,128)(2,1)S(1)} %copy-done.4), kind=kOutput, calls=%fused_computation.14 | convolution fusion | flops 16834560 | bytes 1146880 | tf_op jit(solution)/shard_map/dot_general | solution.py:137
  61.5 10.7 %all_to_all.70 = bf16[16,16,512]{2,1,0:T(8,128)(2,1)S(1)} all-to-all(bf16[16,16,512]{2,1,0:T(8,128)(2,1)S(1)} %broadcast_in_dim.10), channel_id=1, replica_groups=mesh['tp'=16,'dp'=8] {'tp'}, dimensions={0} | all-to-all | bytes 524288 | tf_op jit(solution)/shard_map/all_to_all | solution.py:15
  72.2 0.1 fusion.20
  72.5 0.2 fusion.22
  72.7 0.8 pad_maximum_fusion.2
  73.5 7.9 %all-to-all-start.5 = ((f32[8,32,65]{2,1,0:T(8,128)}), f32[8,32,65]{2,1,0:T(8,128)S(1)}, u32[]{:S(2)}, u32[]{:S(2)}) async-start(f32[8,32,65]{2,1,0:T(8,128)} %pad_maximum_fusion.2), calls=%async_computation.5 | async-start | bytes 262144 | tf_op jit(solution)/shard_map/all_to_all | solution.py:39
  81.4 5.2 %all-to-all-done.5 = f32[8,32,65]{2,1,0:T(8,128)S(1)} async-done(((f32[8,32,65]{2,1,0:T(8,128)}), f32[8,32,65]{2,1,0:T(8,128)S(1)}, u32[]{:S(2)}, u32[]{:S(2)}) %all-to-all-start.5) | async-done | bytes 66592 | tf_op jit(solution)/shard_map/all_to_all | solution.py:39
  86.6 0.2 fusion.58
  87.0 0.2 convolution_bitcast_fusion
  87.2 0.1 multiply_subtract_fusion
  87.3 0.2 fusion.28
  87.7 0.7 reshape.174
  88.4 4.1 %all-to-all-start.6 = ((bf16[8,2,1024]{2,1,0:T(2,128)(2,1)}), bf16[8,2,1024]{2,1,0:T(2,128)(2,1)S(1)}, u32[]{:S(2)}, u32[]{:S(2)}) async-start(bf16[8,2,1024]{2,1,0:T(2,128)(2,1)} %reshape.174), calls=%async_computation.6 | async-start | bytes 65536 | tf_op jit(solution)/shard_map/all_to_all | solution.py:15
  92.6 4.6 %all-to-all-done.6 = bf16[8,2,1024]{2,1,0:T(2,128)(2,1)S(1)} async-done(((bf16[8,2,1024]{2,1,0:T(2,128)(2,1)}), bf16[8,2,1024]{2,1,0:T(2,128)(2,1)S(1)}, u32[]{:S(2)}, u32[]{:S(2)}) %all-to-all-start.6) | async-done | bytes 32800 | tf_op jit(solution)/shard_map/all_to_all | solution.py:15
  97.3 0.1 reshape.175
  97.4 0.7 reshape.176
  98.1 3.5 %all-to-all-start.7 = ((bf16[16,2,512]{2,1,0:T(2,128)(2,1)}), bf16[16,2,512]{2,1,0:T(2,128)(2,1)S(1)}, u32[]{:S(2)}, u32[]{:S(2)}) async-start(bf16[16,2,512]{2,1,0:T(2,128)(2,1)} %reshape.176), calls=%async_computation.7 | async-start | bytes 65536 | tf_op jit(solution)/shard_map/all_to_all | solution.py:134
  101.6 0.7 copy.56
  102.4 5.6 %all-to-all-done.7 = bf16[16,2,512]{2,1,0:T(2,128)(2,1)S(1)} async-done(((bf16[16,2,512]{2,1,0:T(2,128)(2,1)}), bf16[16,2,512]{2,1,0:T(2,128)(2,1)S(1)}, u32[]{:S(2)}, u32[]{:S(2)}) %all-to-all-start.7) | async-done | bytes 32800 | tf_op jit(solution)/shard_map/all_to_all | solution.py:134
  108.0 0.1 reshape.177
  108.1 0.1 all_to_all.59
  108.3 1.5 %fusion.13 = f32[16,512]{1,0:T(8,128)S(1)} fusion(bf16[16,1024]{1,0:T(8,128)(2,1)S(1)} %all_to_all.59, bf16[1024,1024]{1,0:T(8,128)(2,1)} %all-gather.5.cloned.1.call-done), kind=kOutput, calls=%fused_computation.17 | convolution fusion | flops 16777216 | bytes 1114112 | tf_op jit(solution)/shard_map/dot_general | solution.py:136
  109.7 2.1 %fusion.11 = bf16[16,512]{1,0:T(8,128)(2,1)} fusion(f32[16,512]{1,0:T(8,128)S(1)} %fusion.13, bf16[16,1024]{1,0:T(8,128)(2,1)S(1)} %all_to_all.59, bf16[1024,1024]{1,0:T(8,128)(2,1)} %all-gather.5.cloned.1.call-done, bf16[16,512]{1,0:T(8,128)(2,1)S(1)} %fusion.10), kind=kOutput, calls=%fused_computation.15 | convolution fusion | flops 16834560 | bytes 1146880 | tf_op jit(solution)/shard_map/dot_general | solution.py:137
  (52 shorter events, 1.4 us)
Async XLA Ops:
  7.2 12.8 %copy-start.8 = (f32[2,4]{1,0:T(2,128)S(1)}, f32[2,4]{1,0:T(2,128)}, u32[]{:S(2)}) copy-start(f32[2,4]{1,0:T(2,128)} %param.17) | copy-start | bytes 100
  7.2 12.8 %copy-start.1 = (f32[2,32,4,128]{3,2,1,0:T(4,128)S(1)}, f32[2,32,4,128]{3,2,1,0:T(4,128)}, u32[]{:S(2)}) copy-start(f32[2,32,4,128]{3,2,1,0:T(4,128)} %param.23) | copy-start | bytes 393220
  7.2 12.9 %copy-start.5 = (f32[2,4,64]{2,1,0:T(4,128)S(1)}, f32[2,4,64]{2,1,0:T(4,128)}, u32[]{:S(2)}) copy-start(f32[2,4,64]{2,1,0:T(4,128)} %param.15) | copy-start | bytes 6148
  7.2 12.9 %copy-start.6 = (f32[2,4,64]{2,1,0:T(4,128)S(1)}, f32[2,4,64]{2,1,0:T(4,128)}, u32[]{:S(2)}) copy-start(f32[2,4,64]{2,1,0:T(4,128)} %param.16) | copy-start | bytes 6148
  7.2 13.1 %copy-start.7 = (f32[2,512]{1,0:T(2,128)S(1)}, f32[2,512]{1,0:T(2,128)}, u32[]{:S(2)}) copy-start(f32[2,512]{1,0:T(2,128)} %param.13) | copy-start | bytes 12292
  7.2 19.8 %copy-start = (bf16[2,512,64]{1,2,0:T(8,128)(2,1)S(1)}, bf16[2,512,64]{1,2,0:T(8,128)(2,1)}, u32[]{:S(2)}) copy-start(bf16[2,512,64]{1,2,0:T(8,128)(2,1)} %param.14) | copy-start | bytes 393220
  7.2 51.3 %all-gather.3.cloned.1.call-start = ((), (), s32[]{:S(2)}) async-start(), calls=%async_computation.8 | async-start | bytes 2228224 | tf_op jit(solution)/shard_map/all_gather | solution.py:60
  8.3 26.1 %copy-start.9 = (f32[2,64]{1,0:T(2,128)S(1)}, f32[2,64]{1,0:T(2,128)}, u32[]{:S(2)}) copy-start(f32[2,64]{1,0:T(2,128)} %param.20) | copy-start | bytes 1540
  8.3 31.7 %copy-start.2 = (f32[2,4,16,128]{3,2,1,0:T(8,128)S(1)}, f32[2,4,16,128]{3,2,1,0:T(8,128)}, u32[]{:S(2)}) copy-start(f32[2,4,16,128]{3,2,1,0:T(8,128)} %param.18) | copy-start | bytes 196612
  10.5 29.9 %copy-start.3 = (f32[2,4,16,128]{3,2,1,0:T(8,128)S(1)}, f32[2,4,16,128]{3,2,1,0:T(8,128)}, u32[]{:S(2)}) copy-start(f32[2,4,16,128]{3,2,1,0:T(8,128)} %param.19) | copy-start | bytes 196612
  10.5 16.3 %all-to-all-start = ((bf16[16,16,512]{2,1,0:T(8,128)(2,1)}), bf16[16,16,512]{2,1,0:T(8,128)(2,1)S(1)}, u32[]{:S(2)}, u32[]{:S(2)}) async-start(bf16[16,16,512]{2,1,0:T(8,128)(2,1)} %broadcast_in_dim.8), calls=%async_computation | async-start | bytes 524288 | tf_op jit(solution)/shard_map/all_to_all | solution.py:15
  19.2 89.0 %all-gather.5.cloned.1.call-start = ((), (), s32[]{:S(2)}) async-start(), calls=%async_computation.9 | async-start | bytes 2228224 | tf_op jit(solution)/shard_map/all_gather | solution.py:60
  26.9 33.0 %copy-start.4 = (bf16[16,512]{1,0:T(8,128)(2,1)S(1)}, bf16[16,512]{1,0:T(8,128)(2,1)}, u32[]{:S(2)}) copy-start(bf16[16,512]{1,0:T(8,128)(2,1)} %param.12) | copy-start | bytes 49156
  28.0 11.6 %all-to-all-start.1 = ((f32[8,32,65]{2,1,0:T(8,128)}), f32[8,32,65]{2,1,0:T(8,128)S(1)}, u32[]{:S(2)}, u32[]{:S(2)}) async-start(f32[8,32,65]{2,1,0:T(8,128)} %pad_maximum_fusion), calls=%async_computation.1 | async-start | bytes 262144 | tf_op jit(solution)/shard_map/all_to_all | solution.py:39
  73.5 13.1 %all-to-all-start.5 = ((f32[8,32,65]{2,1,0:T(8,128)}), f32[8,32,65]{2,1,0:T(8,128)S(1)}, u32[]{:S(2)}, u32[]{:S(2)}) async-start(f32[8,32,65]{2,1,0:T(8,128)} %pad_maximum_fusion.2), calls=%async_computation.5 | async-start | bytes 262144 | tf_op jit(solution)/shard_map/all_to_all | solution.py:39
  88.4 8.8 %all-to-all-start.6 = ((bf16[8,2,1024]{2,1,0:T(2,128)(2,1)}), bf16[8,2,1024]{2,1,0:T(2,128)(2,1)S(1)}, u32[]{:S(2)}, u32[]{:S(2)}) async-start(bf16[8,2,1024]{2,1,0:T(2,128)(2,1)} %reshape.174), calls=%async_computation.6 | async-start | bytes 65536 | tf_op jit(solution)/shard_map/all_to_all | solution.py:15
  98.1 9.9 %all-to-all-start.7 = ((bf16[16,2,512]{2,1,0:T(2,128)(2,1)}), bf16[16,2,512]{2,1,0:T(2,128)(2,1)S(1)}, u32[]{:S(2)}, u32[]{:S(2)}) async-start(bf16[16,2,512]{2,1,0:T(2,128)(2,1)} %reshape.176), calls=%async_computation.7 | async-start | bytes 65536 | tf_op jit(solution)/shard_map/all_to_all | solution.py:134
Sparse Core Ops, SparseCore 0:
  10.2 46.8 all-gather.2
  59.2 44.4 all-gather.4
where the time goes:
time: 120 us; the launch traced here: 119 us
  starting transfers between devices  30.7 us (26%)
  blocking collectives  27.8 us (23%)
  waiting for transfers between devices  27.2 us (23%)
  between operations  14.4 us (12%)
  matrix products  7.75 us (6%)
  local copies, waits for them, and re-layouts  6.27 us (5%)
  other arithmetic  4.54 us (4%)
    all_to_all x2, blocking collectives, copy_for_each(): lax.all_to_all(jnp.broadcast_to(shard[None], (devices, *shard.shape)), ax...  18.7 us
    all_to_all x2, starting transfers between devices, sent_and_summed(): lax.all_to_all(split_up(shard, dim, devices), axis, 0, 0, tiled=True)  14.3 us
    all_to_all x2, starting transfers between devices, copy_for_each(): lax.all_to_all(jnp.broadcast_to(shard[None], (devices, *shard.shape)), ax...  12.8 us
    all_to_all x2, waiting for transfers between devices, copy_for_each(): lax.all_to_all(jnp.broadcast_to(shard[None], (devices, *shard.shape)), ax...  11.1 us
    all_to_all x2, waiting for transfers between devices, sent_and_summed(): lax.all_to_all(split_up(shard, dim, devices), axis, 0, 0, tiled=True)  10.4 us
    all_to_all x1, blocking collectives, body(): mixed = lax.all_to_all(ready, 'tp', split_axis=0, concat_axis=1, tiled=True)  9.11 us
    all_to_all x1, waiting for transfers between devices, body(): mixed = lax.all_to_all(ready, 'tp', split_axis=0, concat_axis=1, tiled=True)  5.63 us
    dot_general x2, matrix products, body(): gate = jnp.dot(mixed, pieces[1], preferred_element_type=jnp.float32)  3.62 us
  transfers between devices with their start and end apart: 7, of which 5 were waited for; matrix products, arithmetic and copies ran while one was open for 11% of the time, Pallas kernels for 0%

commit v1 on v0

v1 whole, which is shorter than its diff:
```python
import jax
import jax.numpy as jnp
from jax import lax
from jax.experimental import pallas as pl
from jax.experimental.pallas import tpu as pltpu
from jax.sharding import PartitionSpec as P

D = 4096
L = 2
EPS = 1e-06
MESH = pl.DeviceIdType.MESH
F32 = jnp.float32
BF16 = jnp.bfloat16
HIGH = lax.Precision.HIGHEST


def nt(a, b, precision=None):
    return lax.dot_general(
        a, b, (((1,), (1,)), ((), ())), precision=precision, preferred_element_type=F32
    )


def device(z, y, x, c):
    return (z * 4 + y, x * 2 + c)


class Sends:
    def __init__(self):
        self.waits = []

    def go(self, src, dst, send_sem, recv_sem, to, here=None):
        copy = pltpu.make_async_remote_copy(
            src_ref=src, dst_ref=dst, send_sem=send_sem, recv_sem=recv_sem,
            device_id=to, device_id_type=MESH,
        )
        if here is None:
            copy.start()
            self.waits.append((None, copy))
            return

        @pl.when(here)
        def _():
            pltpu.make_async_copy(src, dst, recv_sem).start()

        @pl.when(jnp.logical_not(here))
        def _():
            copy.start()

        self.waits.append((jnp.logical_not(here), copy))

    def finish(self):
        for away, copy in self.waits:
            if away is None:
                copy.wait_send()
            else:
                @pl.when(away)
                def _(copy=copy):
                    copy.wait_send()


def arrived(dst, sem):
    pltpu.make_async_copy(dst, dst, sem).wait()


def kernel(
    tok, gain, win, decay, freq, step, sin, rdo, skip, wv, wg, st,
    tok_out, st_out,
    xg, wi, wo, gain_v, decay_v, freq_v, step_v, sin_v, rdo_v, skip_v, st_v,
    big_b, m3, base, ks, pb, sq, bm, bq, cs, cr, part, rs, rr, new_v, out_v,
    load, load_w, load_o, load_st, a_s, a_r, w_s, w_r, o_s, o_r,
    b_s, b_r, q_s, q_r, c_s, c_r, r_s, r_r, done,
):
    t, d = lax.axis_index("tp"), lax.axis_index("dp")
    z, y, x, c = t // 4, t % 4, d // 2, d % 2
    barrier = pltpu.get_barrier_semaphore()
    greeted = [(z, (y + i) % 4, x, c) for i in (1, 2, 3)]
    greeted += [((z + i) % 4, y, x, c) for i in (1, 2, 3)]
    greeted += [(z, y, (x + i) % 4, (c + k) % 2) for i in range(4) for k in range(2) if i + k]
    for peer in greeted:
        pl.semaphore_signal(barrier, inc=1, device_id=device(*peer), device_id_type=MESH)

    loads = [
        pltpu.make_async_copy(tok, xg.at[0, y], a_r.at[0, y]),
        pltpu.make_async_copy(win.at[0], wi.at[0, 0], load_w.at[0]),
    ]
    small = [(decay, decay_v), (freq, freq_v), (step, step_v), (sin, sin_v), (rdo, rdo_v),
             (skip, skip_v), (gain, gain_v)]
    small_loads = [
        pltpu.make_async_copy(src, dst, load.at[i]) for i, (src, dst) in enumerate(small)
    ]
    st_load = pltpu.make_async_copy(st, st_v, load_st.at[0])
    wo_loads = []
    for l in range(L):
        for k, w in enumerate((wv, wg)):
            wo_loads.append(pltpu.make_async_copy(w.at[l], wo.at[l, y, k], load_o.at[l, k]))
    w1_load = pltpu.make_async_copy(win.at[1], wi.at[1, 0], load_w.at[1])
    for copy in loads + wo_loads[:2] + small_loads + [st_load, w1_load] + wo_loads[2:]:
        copy.start()

    sends = Sends()

    loads[1].wait()
    loads[0].wait()
    pl.semaphore_wait(barrier, len(greeted))

    def send_x(l):
        for i in (1, 3, 2):
            sends.go(xg.at[l, y], xg.at[l, y], a_s.at[l, i], a_r.at[l, y],
                     device(z, (y + i) % 4, x, c))

    def send_win(l):
        for i in (2, 1, 3):
            sends.go(wi.at[l, 0], wi.at[l, i], w_s.at[l, i], w_r.at[l, i],
                     device((z + i) % 4, y, x, c))

    def send_wo(l):
        for i in (1, 3, 2):
            sends.go(wo.at[l, y], wo.at[l, y], o_s.at[l, i], o_r.at[l, y],
                     device(z, (y + i) % 4, x, c))

    send_x(0)
    send_win(0)
    wo_loads[0].wait()
    wo_loads[1].wait()
    send_wo(0)

    for copy in small_loads:
        copy.wait()
    rate = jnp.concatenate([decay_v[0], decay_v[1]], axis=0)
    often = jnp.concatenate([freq_v[0], freq_v[1]], axis=0)
    steps = step_v[...]
    times = jnp.concatenate(
        [jnp.broadcast_to(steps[l:l + 1, g:g + 1], (1, 64)) for l in range(L) for g in range(4)],
        axis=0,
    )
    magnitude = jnp.exp(-rate * times)
    angle = often * times
    keep_r = magnitude * jnp.cos(angle)
    keep_i = magnitude * jnp.sin(angle)
    minus = keep_r - 1.0
    below = rate * rate + often * often
    lift_r = (-minus * rate + keep_i * often) / below
    lift_i = (-keep_i * rate - minus * often) / below
    keep_r = jnp.concatenate([keep_r, keep_r], axis=1)
    keep_i = jnp.concatenate([-keep_i, keep_i], axis=1)
    lift_r = jnp.concatenate([lift_r, lift_r], axis=1)
    lift_i = jnp.concatenate([-lift_i, lift_i], axis=1)

    rows = lax.broadcasted_iota(jnp.int32, (128, 128), 0)
    lanes = lax.broadcasted_iota(jnp.int32, (128, 128), 1)
    same_group = rows // 16 == lanes // 16
    lane16 = lax.broadcasted_iota(jnp.int32, (16, 128), 1)
    row16 = lax.broadcasted_iota(jnp.int32, (16, 128), 0)
    low = lane16 < 64

    st_load.wait()
    for l in range(L):
        lifted = []
        for g in range(4):
            k = l * 4 + g
            b = sin_v[l, g]
            lifted.append(lift_r[k:k + 1] * b + lift_i[k:k + 1] * pltpu.roll(b, 64, 1))
        both = jnp.concatenate(lifted + lifted, axis=0)
        big_b[l] = both
        out = jnp.concatenate([rdo_v[l, g] for g in range(4)] * 2, axis=0)
        skips = jnp.concatenate([skip_v[l:l + 1], skip_v[l:l + 1]], axis=1)
        m = jnp.where(same_group, nt(both, out, HIGH), 0.0)
        m = m + jnp.where(rows == lanes, jnp.broadcast_to(skips, (128, 128)), 0.0)
        hi = m.astype(BF16)
        m3[l] = jnp.concatenate([hi, hi, (m - hi.astype(F32)).astype(BF16)], axis=0)
        for g in range(4):
            k = l * 4 + g
            s = st_v[l, :, g, :]
            kept = keep_r[k:k + 1] * s + keep_i[k:k + 1] * pltpu.roll(s, 64, 1)
            ks[l, g * 2] = kept[:16]
            ks[l, g * 2 + 1] = kept[16:]
        prod = nt(ks[l].reshape(128, 128), out, HIGH)
        total = jnp.zeros((16, 128), F32)
        for g in range(4):
            for h in range(2):
                block = prod[(g * 2 + h) * 16:(g * 2 + h) * 16 + 16]
                total = total + jnp.where(lane16 // 16 == h * 4 + g, block, 0.0)
        base[l] = total

    w1_load.wait()

    for l in range(L):
        for k in range(4):
            @pl.when(y != k)
            def _(k=k):
                arrived(xg.at[l, k], a_r.at[l, k])
        wide = xg[l].reshape(64, 512).astype(F32)
        gained = (wide * gain_v[l:l + 1]).astype(BF16)
        square = jnp.sum(wide * wide, axis=1, keepdims=True)
        row32 = lax.broadcasted_iota(jnp.int32, (32, 128), 0)
        lane32 = lax.broadcasted_iota(jnp.int32, (32, 128), 1)
        for k in range(2):
            part_sq = jnp.where(row32 == lane32, square[k * 32:k * 32 + 32], 0.0)
            sq[l, k] = jnp.broadcast_to(jnp.sum(part_sq, axis=0, keepdims=True), (8, 128))
        for i in (0, 1, 3, 2):
            if i:
                arrived(wi.at[l, i], w_r.at[l, i])
            twice = jnp.concatenate([wi[l, i], wi[l, i]], axis=0)
            prod = nt(gained, twice)
            zz = (z - i) % 4
            for k in range(2):
                a = prod[k * 32:k * 32 + 16]
                b = prod[k * 32 + 16:k * 32 + 32]
                pb[l, i, k] = jnp.where(low, a, b).astype(BF16)
            for k in range(2):
                to = device(zz, y, z, k)
                here = None if i else jnp.logical_and(x == z, c == k)
                slot = x * 2 + c
                sends.go(pb.at[l, i, k], bm.at[l, slot], b_s.at[l, i * 2 + k], b_r.at[l, slot],
                         to, here)
                sends.go(sq.at[l, k], bq.at[l, slot], q_s.at[l, i * 2 + k], q_r.at[l, slot],
                         to, here)
        if l == 0:
            send_win(1)

        for k in range(8):
            arrived(bq.at[l, k], q_r.at[l, k])
            arrived(bm.at[l, k], b_r.at[l, k])
        squares = bq[l, 0]
        raw = bm[l, 0].astype(F32)
        for k in range(1, 8):
            squares = squares + bq[l, k]
            raw = raw + bm[l, k].astype(F32)
        hi = raw.astype(BF16)
        lo = (raw - hi.astype(F32)).astype(BF16)
        mixed = jnp.dot(
            jnp.concatenate([hi, lo, hi], axis=1), m3[l], preferred_element_type=F32
        )
        spread = jnp.broadcast_to(squares[0:1], (16, 128))
        first = jnp.sum(jnp.where(lane16 == row16, spread, 0.0), axis=1, keepdims=True)
        second = jnp.sum(jnp.where(lane16 == row16 + 16, spread, 0.0), axis=1, keepdims=True)
        scale = lax.rsqrt(jnp.where(low, first, second) * (1.0 / D) + EPS)
        ready = jax.nn.gelu(base[l] + scale * mixed)
        turned = pltpu.roll(ready, 64, 1)
        side = y % 2
        for h in range(2):
            placed = jnp.where(side == h, ready, turned)
            cs[l, h] = jnp.where(lane16 // 64 == side, placed, 0.0).astype(BF16)
        for h in range(2):
            yy = 2 * c + h
            for i in (2, 1, 3, 0):
                for k in range(2):
                    here = y == yy if i + k == 0 else None
                    sends.go(cs.at[l, h], cr.at[l, x, y], c_s.at[l, h * 8 + i * 2 + k],
                             c_r.at[l, x, y], device(z, yy, (x + i) % 4, (c + k) % 2), here)
        if l == 0:
            wo_loads[2].wait()
            wo_loads[3].wait()
            send_wo(1)

        drive = scale * raw
        pieces = [
            jnp.where(lane16 // 16 == h * 4 + g, drive, 0.0) for g in range(4) for h in range(2)
        ]
        push = jnp.dot(
            jnp.concatenate(pieces, axis=0), big_b[l], precision=HIGH, preferred_element_type=F32
        )
        for g in range(4):
            for h in range(2):
                k = g * 2 + h
                new_v[l, h * 16:h * 16 + 16, g, :] = ks[l, k] + push[k * 16:k * 16 + 16]
        pltpu.make_async_copy(new_v.at[l], st_out.at[l], done.at[l]).start()

        for k in range(4):
            @pl.when(y != k)
            def _(k=k):
                arrived(wo.at[l, k], o_r.at[l, k])
        for i in range(4):
            for k in range(4):
                arrived(cr.at[l, i, k], c_r.at[l, i, k])
        left = jnp.concatenate(
            [
                (cr[l, :, 2 * j] + cr[l, :, 2 * j + 1]).reshape(64, 128)
                for j in range(2)
            ],
            axis=1,
        )
        for k in range(2):
            prod = jnp.dot(left, wo[l, :, k].reshape(256, 512), preferred_element_type=F32)
            for i in range(4):
                part[l, i, k] = prod[i * 16:i * 16 + 16]
                rs[l, i, k] = prod[i * 16:i * 16 + 16].astype(BF16)
        for i in (2, 1, 3):
            zz = (z + i) % 4
            sends.go(rs.at[l, zz], rr.at[l, i], r_s.at[l, i], r_r.at[l, i], device(zz, y, x, c))
        value, gate = part[l, z, 0], part[l, z, 1]
        for i in (1, 3, 2):
            arrived(rr.at[l, i], r_r.at[l, i])
            value = value + rr[l, i, 0].astype(F32)
            gate = gate + rr[l, i, 1].astype(F32)
        current = (xg[l, y].astype(F32) + value * jax.nn.sigmoid(gate)).astype(BF16)
        if l + 1 < L:
            xg[l + 1, y] = current
            send_x(l + 1)
        else:
            out_v[...] = current
            copy = pltpu.make_async_copy(out_v, tok_out, done.at[L])
            copy.start()
            copy.wait()
    sends.finish()
    for l in range(L):
        pltpu.make_async_copy(new_v.at[l], st_out.at[l], done.at[l]).wait()


def body(*args):
    args = list(args)
    args[2] = jnp.swapaxes(args[2], 1, 2)
    dma = pltpu.SemaphoreType.DMA
    v = pltpu.VMEM
    anywhere = pl.BlockSpec(memory_space=pl.ANY)
    scratch = [
        v((L, 4, 16, 512), BF16),
        v((L, 4, 64, 512), BF16),
        v((L, 4, 2, 64, 512), BF16),
        v((L, 512), F32),
        v((L, 4, 64), F32),
        v((L, 4, 64), F32),
        v((L, 4), F32),
        v((L, 4, 16, 128), F32),
        v((L, 4, 16, 128), F32),
        v((L, 64), F32),
        v((L, 32, 4, 128), F32),
        v((L, 128, 128), F32),
        v((L, 384, 128), BF16),
        v((L, 16, 128), F32),
        v((L, 8, 16, 128), F32),
        v((L, 4, 2, 16, 128), BF16),
        v((L, 2, 8, 128), F32),
        v((L, 8, 16, 128), BF16),
        v((L, 8, 8, 128), F32),
        v((L, 2, 16, 128), BF16),
        v((L, 4, 4, 16, 128), BF16),
        v((L, 4, 2, 16, 512), F32),
        v((L, 4, 2, 16, 512), BF16),
        v((L, 4, 2, 16, 512), BF16),
        v((L, 32, 4, 128), F32),
        v((16, 512), BF16),
        dma((7,)), dma((L,)), dma((L, 2)), dma((1,)),
        dma((L, 4)), dma((L, 4)),
        dma((L, 4)), dma((L, 4)),
        dma((L, 4)), dma((L, 4)),
        dma((L, 8)), dma((L, 8)),
        dma((L, 8)), dma((L, 8)),
        dma((L, 16)), dma((L, 4, 4)),
        dma((L, 4)), dma((L, 4)),
        dma((L + 1,)),
    ]
    return pl.pallas_call(
        kernel,
        out_shape=(
            jax.ShapeDtypeStruct((16, 512), BF16),
            jax.ShapeDtypeStruct((L, 32, 4, 128), F32),
        ),
        in_specs=[anywhere] * 12,
        out_specs=(anywhere, anywhere),
        scratch_shapes=scratch,
        compiler_params=pltpu.CompilerParams(collective_id=0, has_side_effects=True),
        name="layers",
    )(*args)


def solution(mesh):
    in_specs = (
        P("tp", "dp"),
        P(None, "dp"),
        P(None, "dp", "tp"),
        P(None, "tp", None),
        P(None, "tp", None),
        P(None, "tp"),
        P(None, "tp", None, None),
        P(None, "tp", None, None),
        P(None, "tp"),
        P(None, "tp", "dp"),
        P(None, "tp", "dp"),
        P(None, "dp", "tp", None),
    )
    out_specs = (P("tp", "dp"), P(None, "dp", "tp", None))
    return jax.shard_map(body, mesh=mesh, in_specs=in_specs, out_specs=out_specs, check_vma=False)
```

time: 120 us -> 50.6 us (0.42)
  Pallas kernels: 0 us -> 46.8 us
  starting transfers between devices: 30.7 us -> 0 us
  blocking collectives: 27.8 us -> 0 us
  waiting for transfers between devices: 27.2 us -> 0 us
  between operations: 14.4 us -> 0.64 us
  matrix products: 7.75 us -> 0 us
  other arithmetic: 4.54 us -> 0 us
  local copies, waits for them, and re-layouts: 6.27 us -> 2.89 us
    pallas_call x0 -> x1, Pallas kernels: none -> 46.8 us  [body(): pl.pallas_call(kernel, out_shape=(jax.ShapeDtypeStruct((16, 512), BF16),...]
    all_to_all x5 -> x0, starting transfers between devices: 30.6 us -> none  [the longest x2 14.3 us: sent_and_summed(): lax.all_to_all(split_up(shard, dim, devices), axis, 0, 0, tiled=True)]
    all_to_all x3 -> x0, blocking collectives: 27.8 us -> none  [the longest x2 18.7 us: copy_for_each(): lax.all_to_all(jnp.broadcast_to(shard[None], (devices, *shard.shape)), ax...]
    all_to_all x5 -> x0, waiting for transfers between devices: 27.1 us -> none  [the longest x2 11.1 us: copy_for_each(): lax.all_to_all(jnp.broadcast_to(shard[None], (devices, *shard.shape)), ax...]
    dot_general x10 -> x0, matrix products: 7.75 us -> none  [the longest x2 3.62 us: body(): gate = jnp.dot(mixed, pieces[1], preferred_element_type=jnp.float32)]
    concatenate x4 -> x0, other arithmetic: 2.85 us -> none  [the longest x2 1.52 us: in_one_piece(): both = jnp.concatenate(columns, axis=along)]
    broadcast_in_dim x4 -> x0, local copies, waits for them, and re-layouts: 1.51 us -> none  [copy_for_each(): jnp.broadcast_to(shard[None], (devices, *shard.shape))]
    unnamed x29 -> x2, local copies, waits for them, and re-layouts: 2.9 us -> 2.89 us
  transfers between devices with their start and end apart: 7 -> 0, of which waited for: 5 -> 0; matrix products, arithmetic and copies ran while one was open for 11% -> 0% of each run, Pallas kernels for 0% -> 0%
where the time goes in v1:
time: 50.6 us; the launch traced here: 50.4 us
  Pallas kernels  46.8 us (92%)
  local copies, waits for them, and re-layouts  2.89 us (6%)
  between operations  0.64 us (1%)
    pallas_call x1, Pallas kernels, body(): pl.pallas_call(kernel, out_shape=(jax.ShapeDtypeStruct((16, 512), BF16),...  46.8 us
    unnamed x2, local copies, waits for them, and re-layouts  2.89 us

profile of v1, /device:TPU:1, one launch (start us, length us, event | category | flops | bytes accessed | tf_op | source)
XLA Modules:
  0.0 50.4 jit_solution(3860543778619951391)
XLA Ops:
  0.6 46.8 %layers.1 = (bf16[16,512]{1,0:T(8,128)(2,1)}, f32[2,32,4,128]{3,2,1,0:T(4,128)}) custom-call(bf16[16,512]{1,0:T(8,128)(2,1)} %tok.1, f32[2,512]{1,0:T(2,128)} %gain.1, bf16[2,64,512]{2,1,0:T(8,128)(2,1)} %bitcast.1, f32[2,4,64]{2,1,0:T(4,128)} %decay.1, f32[2,4,64]{2,1,0:T(4,128)} %freq.1, f32[2,4]{1,0:T(2,128)} %step.1, f32[2,4,16,128]{3,2,1,0:T(8,128)} %sin.1, ...), custom_call_target="tpu_custom_call" | custom-call | tf_op jit(solution)/shard_map/layers/pallas_call | solution.py:353
  47.5 1.3 %copy.16 = bf16[16,512]{1,0:T(8,128)(2,1)} copy(bf16[16,512]{1,0:T(8,128)(2,1)} %get-tuple-element.4) | data formatting | bytes 32768
  48.8 1.6 %copy.17 = f32[2,32,4,128]{3,2,1,0:T(4,128)} copy(f32[2,32,4,128]{3,2,1,0:T(4,128)} %get-tuple-element.5) | data formatting | bytes 262144

commit v2 on v1

v2 whole, which is shorter than its diff:
```python
import jax
import jax.numpy as jnp
from jax import lax
from jax.experimental import pallas as pl
from jax.experimental.pallas import tpu as pltpu
from jax.sharding import PartitionSpec as P

D = 4096
L = 2
EPS = 1e-06
MESH = pl.DeviceIdType.MESH
F32 = jnp.float32
BF16 = jnp.bfloat16
HIGH = lax.Precision.HIGHEST


def nt(a, b, precision=None):
    return lax.dot_general(
        a, b, (((1,), (1,)), ((), ())), precision=precision, preferred_element_type=F32
    )


def device(z, y, x, c):
    return (z * 4 + y, x * 2 + c)


class Sends:
    def __init__(self):
        self.waits = []

    def go(self, src, dst, send_sem, recv_sem, to, here=None):
        copy = pltpu.make_async_remote_copy(
            src_ref=src, dst_ref=dst, send_sem=send_sem, recv_sem=recv_sem,
            device_id=to, device_id_type=MESH,
        )
        if here is None:
            copy.start()
            self.waits.append((None, copy))
            return

        @pl.when(here)
        def _():
            pltpu.make_async_copy(src, dst, recv_sem).start()

        @pl.when(jnp.logical_not(here))
        def _():
            copy.start()

        self.waits.append((jnp.logical_not(here), copy))

    def finish(self):
        for away, copy in self.waits:
            if away is None:
                copy.wait_send()
            else:
                @pl.when(away)
                def _(copy=copy):
                    copy.wait_send()


def arrived(dst, sem):
    pltpu.make_async_copy(dst, dst, sem).wait()


def kernel(
    tok, gain, win, decay, freq, step, sin, rdo, skip, wv, wg, st,
    tok_out, st_out,
    xg, wi, wt, w_raw, w0, wo, gain_v, gain_all, decay_v, freq_v, step_v, sin_v, rdo_v, skip_v, st_v,
    big_b, m3, base, ks, pb, sq, bm, bq, rg, res0, xa, res1, cs, cr, part, rs, rr, new_v, out_v,
    load, load_st, load_w, load_o, load_x, a_s, a_r, w_s, w_r, o_s, o_r,
    b_s, b_r, q_s, q_r, c_s, c_r, r_s, r_r, t_s, t_r, tf_s, g_s, g_r, h_s, h_r, hf_s,
    k_s, k_r, n_s, n_r, e_s, e_r, near_sem, far_sem, done,
):
    t, d = lax.axis_index("tp"), lax.axis_index("dp")
    z, y, x, c = t // 4, t % 4, d // 2, d % 2
    other = 1 - c
    barrier = pltpu.get_barrier_semaphore()
    greeted = [(z, (y + i) % 4, x, c) for i in (1, 2, 3)]
    greeted += [((z + i) % 4, y, x, c) for i in (1, 2, 3)]
    greeted += [(z, y, (x + i) % 4, (c + k) % 2) for i in range(4) for k in range(2) if i + k]
    for peer in greeted:
        pl.semaphore_signal(barrier, inc=1, device_id=device(*peer), device_id_type=MESH)

    tok_load = pltpu.make_async_copy(tok, xg.at[y], load_x.at[0])
    win_loads = [
        pltpu.make_async_copy(win.at[0], wi.at[0], load_w.at[0]),
        pltpu.make_async_copy(win.at[1], wt.at[d], load_w.at[1]),
    ]
    raw_loads = [
        pltpu.make_async_copy(w.at[0], w_raw.at[k], load_o.at[0, k]) for k, w in enumerate((wv, wg))
    ]
    wo_loads = [
        pltpu.make_async_copy(w.at[1], wo.at[y, k], load_o.at[1, k]) for k, w in enumerate((wv, wg))
    ]
    small = [(decay, decay_v), (freq, freq_v), (step, step_v), (sin, sin_v), (rdo, rdo_v),
             (skip, skip_v)]
    small_loads = [
        pltpu.make_async_copy(src, dst, load.at[i]) for i, (src, dst) in enumerate(small)
    ]
    gain_load = pltpu.make_async_copy(gain, gain_v, load.at[6])
    st_load = pltpu.make_async_copy(st, st_v, load_st.at[0])
    for copy in [win_loads[0], tok_load, win_loads[1], gain_load] + wo_loads + small_loads + [
        st_load
    ] + raw_loads:
        copy.start()

    plane = [(i, k) for i in range(4) for k in range(4) if i + k]
    plane.sort(key=lambda ik: -(min(ik[0], 4 - ik[0]) + min(ik[1], 4 - ik[1])))

    def peer_of(i, k):
        return device((z + i) % 4, (y + k) % 4, x, c)

    sends = Sends()
    win_loads[0].wait()
    tok_load.wait()
    gain_load.wait()
    gain_all[d] = gain_v[1:2]
    pl.semaphore_wait(barrier, len(greeted))

    for i in (2, 1, 3):
        sends.go(wi.at[0], wi.at[i], w_s.at[i], w_r.at[i], device((z + i) % 4, y, x, c))
    for i in (2, 1, 3):
        sends.go(xg.at[y], xg.at[y], a_s.at[i], a_r.at[y], device(z, (y + i) % 4, x, c))
    for i in (2, 1, 3):
        pl.semaphore_signal(near_sem, inc=1, device_id=peer_of(i, 0), device_id_type=MESH)
    win_loads[1].wait()
    for i in (2, 1, 3):
        sends.go(wt.at[d], wt.at[d], t_s.at[i], t_r.at[d], device(z, y, (x + i) % 4, c))
    for i in (2, 1, 3, 0):
        for k in range(2):
            if i + k:
                sends.go(gain_all.at[d], gain_all.at[d], g_s.at[i * 2 + k], g_r.at[d],
                         device(z, y, (x + i) % 4, (c + k) % 2))
    for copy in wo_loads:
        copy.wait()
    for i in (2, 1, 3):
        sends.go(wo.at[y], wo.at[y], o_s.at[i], o_r.at[y], device(z, (y + i) % 4, x, c))

    for copy in small_loads:
        copy.wait()
    rate = jnp.concatenate([decay_v[0], decay_v[1]], axis=0)
    often = jnp.concatenate([freq_v[0], freq_v[1]], axis=0)
    steps = step_v[...]
    times = jnp.concatenate(
        [jnp.broadcast_to(steps[l:l + 1, g:g + 1], (1, 64)) for l in range(L) for g in range(4)],
        axis=0,
    )
    magnitude = jnp.exp(-rate * times)
    angle = often * times
    keep_r = magnitude * jnp.cos(angle)
    keep_i = magnitude * jnp.sin(angle)
    minus = keep_r - 1.0
    below = rate * rate + often * often
    lift_r = (-minus * rate + keep_i * often) / below
    lift_i = (-keep_i * rate - minus * often) / below
    keep_r = jnp.concatenate([keep_r, keep_r], axis=1)
    keep_i = jnp.concatenate([-keep_i, keep_i], axis=1)
    lift_r = jnp.concatenate([lift_r, lift_r], axis=1)
    lift_i = jnp.concatenate([-lift_i, lift_i], axis=1)

    rows = lax.broadcasted_iota(jnp.int32, (128, 128), 0)
    lanes = lax.broadcasted_iota(jnp.int32, (128, 128), 1)
    same_group = rows // 16 == lanes // 16
    lane16 = lax.broadcasted_iota(jnp.int32, (16, 128), 1)
    row16 = lax.broadcasted_iota(jnp.int32, (16, 128), 0)
    low = lane16 < 64

    st_load.wait()

    def prepare(l):
        lifted = []
        for g in range(4):
            k = l * 4 + g
            b = sin_v[l, g]
            lifted.append(lift_r[k:k + 1] * b + lift_i[k:k + 1] * pltpu.roll(b, 64, 1))
        both = jnp.concatenate(lifted + lifted, axis=0)
        big_b[l] = both
        out = jnp.concatenate([rdo_v[l, g] for g in range(4)] * 2, axis=0)
        skips = jnp.concatenate([skip_v[l:l + 1], skip_v[l:l + 1]], axis=1)
        m = jnp.where(same_group, nt(both, out, HIGH), 0.0)
        m = m + jnp.where(rows == lanes, jnp.broadcast_to(skips, (128, 128)), 0.0)
        hi = m.astype(BF16)
        m3[l] = jnp.concatenate([hi, hi, (m - hi.astype(F32)).astype(BF16)], axis=0)
        for g in range(4):
            k = l * 4 + g
            s = st_v[l, :, g, :]
            kept = keep_r[k:k + 1] * s + keep_i[k:k + 1] * pltpu.roll(s, 64, 1)
            ks[l, g * 2] = kept[:16]
            ks[l, g * 2 + 1] = kept[16:]
        prod = nt(ks[l].reshape(128, 128), out, HIGH)
        total = jnp.zeros((16, 128), F32)
        for g in range(4):
            for h in range(2):
                block = prod[(g * 2 + h) * 16:(g * 2 + h) * 16 + 16]
                total = total + jnp.where(lane16 // 16 == h * 4 + g, block, 0.0)
        base[l] = total

    prepare(0)
    pl.semaphore_wait(near_sem, 3)
    for i in (2, 1, 3):
        pl.semaphore_signal(far_sem, inc=1, device_id=peer_of(0, i), device_id_type=MESH)
    prepare(1)

    def read_out(l, raw, scale):
        hi = raw.astype(BF16)
        lo = (raw - hi.astype(F32)).astype(BF16)
        mixed = jnp.dot(
            jnp.concatenate([hi, lo, hi], axis=1), m3[l], preferred_element_type=F32
        )
        return jax.nn.gelu(base[l] + scale * mixed)

    def new_states(l, drive):
        pieces = [
            jnp.where(lane16 // 16 == h * 4 + g, drive, 0.0) for g in range(4) for h in range(2)
        ]
        push = jnp.dot(
            jnp.concatenate(pieces, axis=0), big_b[l], precision=HIGH, preferred_element_type=F32
        )
        for g in range(4):
            for h in range(2):
                k = g * 2 + h
                new_v[l, h * 16:h * 16 + 16, g, :] = ks[l, k] + push[k * 16:k * 16 + 16]
        pltpu.make_async_copy(new_v.at[l], st_out.at[l], done.at[l]).start()

    for k in range(4):
        @pl.when(y != k)
        def _(k=k):
            arrived(xg.at[k], a_r.at[k])
    wide = xg[...].reshape(64, 512).astype(F32)
    gained = (wide * gain_v[0:1]).astype(BF16)
    square = jnp.sum(wide * wide, axis=1, keepdims=True)
    row32 = lax.broadcasted_iota(jnp.int32, (32, 128), 0)
    lane32 = lax.broadcasted_iota(jnp.int32, (32, 128), 1)
    for k in range(2):
        part_sq = jnp.where(row32 == lane32, square[k * 32:k * 32 + 32], 0.0)
        sq[k] = jnp.broadcast_to(jnp.sum(part_sq, axis=0, keepdims=True), (8, 128))

    pl.semaphore_wait(far_sem, 3)

    def send_w0(k):
        raw_loads[k].wait()
        for i in (2, 1, 3, 0):
            for j in range(2):
                here = None
                if i == 0:
                    here = (z == x) & (y == 2 * c + j) & (y % 2 == c)
                sends.go(w_raw.at[k, :, pl.ds(j * 256, 256)], w0.at[t, k],
                         h_s.at[k, i * 2 + j], h_r.at[t, k],
                         device(x, 2 * c + j, (x + i) % 4, y % 2), here)

    send_w0(0)
    for i in (0, 1, 3, 2):
        if i:
            arrived(wi.at[i], w_r.at[i])
        prod = nt(gained, jnp.concatenate([wi[i], wi[i]], axis=0))
        for k in range(2):
            upper = prod[k * 32:k * 32 + 16]
            lower = prod[k * 32 + 16:k * 32 + 32]
            pb[i, k] = jnp.where(low, upper, lower).astype(BF16)
        for k in range(2):
            to = device((z - i) % 4, y, z, k)
            here = None if i else (x == z) & (c == k)
            sends.go(pb.at[i, k], bm.at[d], b_s.at[i * 2 + k], b_r.at[d], to, here)
            sends.go(sq.at[k], bq.at[d], q_s.at[i * 2 + k], q_r.at[d], to, here)
    send_w0(1)
    for j in range(2):
        here = (z == x) & (y == 2 * c + j)
        sends.go(xg.at[y, :, pl.ds(j * 256, 256)], res0.at[y % 2], e_s.at[0, j],
                 e_r.at[0, y % 2], device(x, 2 * c + j, z, y // 2), here)
    for i in range(4):
        k = ((x + i) % 4) * 2 + c
        if i:
            arrived(wt.at[k], t_r.at[k])
        sends.go(wt.at[k], wt.at[k], tf_s.at[i], t_r.at[k], device(z, y, x, other))

    for k in range(8):
        arrived(bq.at[k], q_r.at[k])
        arrived(bm.at[k], b_r.at[k])
    squares = bq[0]
    raw = bm[0].astype(F32)
    for k in range(1, 8):
        squares = squares + bq[k]
        raw = raw + bm[k].astype(F32)
    spread = jnp.broadcast_to(squares[0:1], (16, 128))
    first = jnp.sum(jnp.where(lane16 == row16, spread, 0.0), axis=1, keepdims=True)
    second = jnp.sum(jnp.where(lane16 == row16 + 16, spread, 0.0), axis=1, keepdims=True)
    scale = lax.rsqrt(jnp.where(low, first, second) * (1.0 / D) + EPS)
    side = y % 2
    ready = read_out(0, raw, scale)
    rg[t] = jnp.where(side == 0, ready, pltpu.roll(ready, 64, 1)).astype(BF16)
    for i, k in plane:
        sends.go(rg.at[t], rg.at[t], k_s.at[i * 4 + k], k_r.at[t], peer_of(i, k))

    for k in range(2):
        for i in range(8):
            s = (i // 2) * 4 + (i % 2) * 2 + c
            arrived(w0.at[s, k], h_r.at[s, k])
            sends.go(w0.at[s, k], w0.at[s, k], hf_s.at[k, i], h_r.at[s, k],
                     device(z, y, x, other))
    new_states(0, scale * raw)
    for k in range(2):
        for i in range(8):
            s = (i // 2) * 4 + (i % 2) * 2 + other
            arrived(w0.at[s, k], h_r.at[s, k])
    for k in range(2):
        arrived(res0.at[k], e_r.at[0, k])
    for k in range(16):
        @pl.when(t != k)
        def _(k=k):
            arrived(rg.at[k], k_r.at[k])
    chunks = []
    for k in range(0, 16, 2):
        even, odd = rg[k], rg[k + 1]
        top = jnp.where(low, even, odd)
        bottom = jnp.where(low, odd, even)
        bottom = jnp.concatenate([bottom[:, 64:], bottom[:, :64]], axis=1)
        chunks.append(jnp.concatenate([top, bottom], axis=0))
    left = jnp.concatenate(chunks, axis=1)
    value = jnp.dot(left, w0[:, 0].reshape(1024, 256), preferred_element_type=F32)
    gate = jnp.dot(left, w0[:, 1].reshape(1024, 256), preferred_element_type=F32)
    current = res0[...].reshape(32, 256).astype(F32) + value * jax.nn.sigmoid(gate)
    xa[t] = current.astype(BF16)
    for i, k in plane:
        sends.go(xa.at[t], xa.at[t], n_s.at[i * 4 + k], n_r.at[t], peer_of(i, k))
    for j in range(2):
        here = (z == x) & (y == 2 * c + j)
        sends.go(xa.at[t, pl.ds(j * 16, 16)], res1.at[y % 2], e_s.at[1, j],
                 e_r.at[1, y % 2], device(x, 2 * c + j, z, y // 2), here)

    for k in range(8):
        @pl.when(d != k)
        def _(k=k):
            arrived(gain_all.at[k], g_r.at[k])
    for i in range(4):
        arrived(wt.at[2 * i + other], t_r.at[2 * i + other])
    for k in range(16):
        @pl.when(t != k)
        def _(k=k):
            arrived(xa.at[k], n_r.at[k])
    total = jnp.zeros((32, 128), F32)
    square = jnp.zeros((32, 256), F32)
    for k in range(16):
        half = slice((k % 2) * 256, (k % 2) * 256 + 256)
        wide = xa[k].astype(F32)
        square = square + wide * wide
        gained = (wide * gain_all[k // 2, :, half]).astype(BF16)
        w = wt[k // 2, :, half]
        total = total + nt(gained, jnp.concatenate([w, w], axis=0))
    square = jnp.sum(square, axis=1, keepdims=True)
    raw = jnp.where(low, total[:16], total[16:])
    scale = lax.rsqrt(jnp.where(low, square[:16], square[16:]) * (1.0 / D) + EPS)
    ready = read_out(1, raw, scale)
    turned = pltpu.roll(ready, 64, 1)
    for h in range(2):
        placed = jnp.where(side == h, ready, turned)
        cs[h] = jnp.where(lane16 // 64 == side, placed, 0.0).astype(BF16)
    for h in range(2):
        yy = 2 * c + h
        for i in (2, 1, 3, 0):
            for k in range(2):
                here = y == yy if i + k == 0 else None
                sends.go(cs.at[h], cr.at[x, y], c_s.at[h * 8 + i * 2 + k],
                         c_r.at[x, y], device(z, yy, (x + i) % 4, (c + k) % 2), here)
    new_states(1, scale * raw)

    for k in range(4):
        @pl.when(y != k)
        def _(k=k):
            arrived(wo.at[k], o_r.at[k])
    for k in range(2):
        arrived(res1.at[k], e_r.at[1, k])
    for i in range(4):
        for k in range(4):
            arrived(cr.at[i, k], c_r.at[i, k])
    left = jnp.concatenate(
        [(cr[:, 2 * j] + cr[:, 2 * j + 1]).reshape(64, 128) for j in range(2)], axis=1
    )
    for k in range(2):
        prod = jnp.dot(left, wo[:, k].reshape(256, 512), preferred_element_type=F32)
        for i in range(4):
            part[i, k] = prod[i * 16:i * 16 + 16]
            rs[i, k] = prod[i * 16:i * 16 + 16].astype(BF16)
    for i in (2, 1, 3):
        zz = (z + i) % 4
        sends.go(rs.at[zz], rr.at[i], r_s.at[i], r_r.at[i], device(zz, y, x, c))
    value, gate = part[z, 0], part[z, 1]
    for i in (1, 3, 2):
        arrived(rr.at[i], r_r.at[i])
        value = value + rr[i, 0].astype(F32)
        gate = gate + rr[i, 1].astype(F32)
    before = jnp.concatenate([res1[0], res1[1]], axis=1).astype(F32)
    out_v[...] = (before + value * jax.nn.sigmoid(gate)).astype(BF16)
    copy = pltpu.make_async_copy(out_v, tok_out, done.at[L])
    copy.start()
    sends.finish()
    copy.wait()
    for l in range(L):
        pltpu.make_async_copy(new_v.at[l], st_out.at[l], done.at[l]).wait()


def body(*args):
    args = list(args)
    args[2] = jnp.swapaxes(args[2], 1, 2)
    dma = pltpu.SemaphoreType.DMA
    v = pltpu.VMEM
    anywhere = pl.BlockSpec(memory_space=pl.ANY)
    scratch = [
        v((4, 16, 512), BF16),
        v((4, 64, 512), BF16),
        v((8, 64, 512), BF16),
        v((2, 64, 512), BF16),
        v((16, 2, 64, 256), BF16),
        v((4, 2, 64, 512), BF16),
        v((L, 512), F32),
        v((8, 1, 512), F32),
        v((L, 4, 64), F32),
        v((L, 4, 64), F32),
        v((L, 4), F32),
        v((L, 4, 16, 128), F32),
        v((L, 4, 16, 128), F32),
        v((L, 64), F32),
        v((L, 32, 4, 128), F32),
        v((L, 128, 128), F32),
        v((L, 384, 128), BF16),
        v((L, 16, 128), F32),
        v((L, 8, 16, 128), F32),
        v((4, 2, 16, 128), BF16),
        v((2, 8, 128), F32),
        v((8, 16, 128), BF16),
        v((8, 8, 128), F32),
        v((16, 16, 128), BF16),
        v((2, 16, 256), BF16),
        v((16, 32, 256), BF16),
        v((2, 16, 256), BF16),
        v((2, 16, 128), BF16),
        v((4, 4, 16, 128), BF16),
        v((4, 2, 16, 512), F32),
        v((4, 2, 16, 512), BF16),
        v((4, 2, 16, 512), BF16),
        v((L, 32, 4, 128), F32),
        v((16, 512), BF16),
        dma((7,)), dma((1,)), dma((2,)), dma((2, 2)), dma((1,)),
        dma((4,)), dma((4,)),
        dma((4,)), dma((4,)),
        dma((4,)), dma((4,)),
        dma((8,)), dma((8,)),
        dma((8,)), dma((8,)),
        dma((16,)), dma((4, 4)),
        dma((4,)), dma((4,)),
        dma((4,)), dma((8,)), dma((4,)),
        dma((8,)), dma((8,)),
        dma((2, 8)), dma((16, 2)), dma((2, 8)),
        dma((16,)), dma((16,)),
        dma((16,)), dma((16,)),
        dma((2, 2)), dma((2, 2)),
        pltpu.SemaphoreType.REGULAR,
        pltpu.SemaphoreType.REGULAR,
        dma((L + 1,)),
    ]
    return pl.pallas_call(
        kernel,
        out_shape=(
            jax.ShapeDtypeStruct((16, 512), BF16),
            jax.ShapeDtypeStruct((L, 32, 4, 128), F32),
        ),
        in_specs=[anywhere] * 12,
        out_specs=(anywhere, anywhere),
        scratch_shapes=scratch,
        compiler_params=pltpu.CompilerParams(collective_id=0, has_side_effects=True),
        name="layers",
    )(*args)


def solution(mesh):
    in_specs = (
        P("tp", "dp"),
        P(None, "dp"),
        P(None, "dp", "tp"),
        P(None, "tp", None),
        P(None, "tp", None),
        P(None, "tp"),
        P(None, "tp", None, None),
        P(None, "tp", None, None),
        P(None, "tp"),
        P(None, "tp", "dp"),
        P(None, "tp", "dp"),
        P(None, "dp", "tp", None),
    )
    out_specs = (P("tp", "dp"), P(None, "dp", "tp", None))
    return jax.shard_map(body, mesh=mesh, in_specs=in_specs, out_specs=out_specs, check_vma=False)
```

time: 50.6 us -> 51.1 us (level)
  Pallas kernels: 46.8 us -> 47.4 us
    pallas_call x1, Pallas kernels: 46.8 us -> 47.4 us  [body(): pl.pallas_call(kernel, out_shape=(jax.ShapeDtypeStruct((16, 512), BF16),...]
where the time goes in v2:
time: 51.1 us; the launch traced here: 50.9 us
  Pallas kernels  47.4 us (93%)
  local copies, waits for them, and re-layouts  2.89 us (6%)
  between operations  0.64 us (1%)
    pallas_call x1, Pallas kernels, body(): pl.pallas_call(kernel, out_shape=(jax.ShapeDtypeStruct((16, 512), BF16),...  47.4 us
    unnamed x2, local copies, waits for them, and re-layouts  2.89 us

profile of v2, /device:TPU:1, one launch (start us, length us, event | category | flops | bytes accessed | tf_op | source)
XLA Modules:
  0.0 50.9 jit_solution(15166043085027863951)
XLA Ops:
  0.6 47.4 %layers.1 = (bf16[16,512]{1,0:T(8,128)(2,1)}, f32[2,32,4,128]{3,2,1,0:T(4,128)}) custom-call(bf16[16,512]{1,0:T(8,128)(2,1)} %tok.1, f32[2,512]{1,0:T(2,128)} %gain.1, bf16[2,64,512]{2,1,0:T(8,128)(2,1)} %bitcast.1, f32[2,4,64]{2,1,0:T(4,128)} %decay.1, f32[2,4,64]{2,1,0:T(4,128)} %freq.1, f32[2,4]{1,0:T(2,128)} %step.1, f32[2,4,16,128]{3,2,1,0:T(8,128)} %sin.1, ...), custom_call_target="tpu_custom_call" | custom-call | tf_op jit(solution)/shard_map/layers/pallas_call | solution.py:460
  48.1 1.3 %copy.16 = bf16[16,512]{1,0:T(8,128)(2,1)} copy(bf16[16,512]{1,0:T(8,128)(2,1)} %get-tuple-element.4) | data formatting | bytes 32768
  49.4 1.6 %copy.17 = f32[2,32,4,128]{3,2,1,0:T(4,128)} copy(f32[2,32,4,128]{3,2,1,0:T(4,128)} %get-tuple-element.5) | data formatting | bytes 262144

commit v3 on v2

--- a/solution.py
+++ b/solution.py
@@ -62,14 +62,19 @@
     pltpu.make_async_copy(dst, dst, sem).wait()
 
 
+def waited(ref, sem, k):
+    arrived(ref.at[k], sem.at[k])
+    return ref[k]
+
+
 def kernel(
     tok, gain, win, decay, freq, step, sin, rdo, skip, wv, wg, st,
     tok_out, st_out,
-    xg, wi, wt, w_raw, w0, wo, gain_v, gain_all, decay_v, freq_v, step_v, sin_v, rdo_v, skip_v, st_v,
-    big_b, m3, base, ks, pb, sq, bm, bq, rg, res0, xa, res1, cs, cr, part, rs, rr, new_v, out_v,
-    load, load_st, load_w, load_o, load_x, a_s, a_r, w_s, w_r, o_s, o_r,
-    b_s, b_r, q_s, q_r, c_s, c_r, r_s, r_r, t_s, t_r, tf_s, g_s, g_r, h_s, h_r, hf_s,
-    k_s, k_r, n_s, n_r, e_s, e_r, near_sem, far_sem, done,
+    xg, wi, wt, w_raw, wy, wz, w0, wp, gain_p, wo, gain_v, gain_all, decay_v, freq_v, step_v, sin_v, rdo_v, skip_v, st_v,
+    big_b, m3, base, ks, pb, sq, bm, bq, rg, res0, rest, xa, res1, cs, cr, part, rs, rr,
+    load, load_st, load_w, load_o, load_x, load_r, a_s, a_r, w_s, w_r, o_s, o_r,
+    b_s, b_r, q_s, q_r, c_s, c_r, r_s, r_r, t_s, t_r, tf_s, g_s, g_r, h_s, h_r, hf_s, hx_r,
+    k_s, k_r, n_s, n_r, e_s, e_r,
 ):
     t, d = lax.axis_index("tp"), lax.axis_index("dp")
     z, y, x, c = t // 4, t % 4, d // 2, d % 2
@@ -87,7 +92,8 @@
         pltpu.make_async_copy(win.at[1], wt.at[d], load_w.at[1]),
     ]
     raw_loads = [
-        pltpu.make_async_copy(w.at[0], w_raw.at[k], load_o.at[0, k]) for k, w in enumerate((wv, wg))
+        pltpu.make_async_copy(w.at[0, :, pl.ds(i * 128, 128)], w_raw.at[i, k], load_r.at[i * 2 + k])
+        for i in range(4) for k, w in enumerate((wv, wg))
     ]
     wo_loads = [
         pltpu.make_async_copy(w.at[1], wo.at[y, k], load_o.at[1, k]) for k, w in enumerate((wv, wg))
@@ -99,9 +105,9 @@
     ]
     gain_load = pltpu.make_async_copy(gain, gain_v, load.at[6])
     st_load = pltpu.make_async_copy(st, st_v, load_st.at[0])
-    for copy in [win_loads[0], tok_load, win_loads[1], gain_load] + wo_loads + small_loads + [
+    for copy in [win_loads[0], tok_load, gain_load] + raw_loads + [win_loads[1]] + small_loads + [
         st_load
-    ] + raw_loads:
+    ] + wo_loads:
         copy.start()
 
     plane = [(i, k) for i in range(4) for k in range(4) if i + k]
@@ -121,8 +127,11 @@
         sends.go(wi.at[0], wi.at[i], w_s.at[i], w_r.at[i], device((z + i) % 4, y, x, c))
     for i in (2, 1, 3):
         sends.go(xg.at[y], xg.at[y], a_s.at[i], a_r.at[y], device(z, (y + i) % 4, x, c))
-    for i in (2, 1, 3):
-        pl.semaphore_signal(near_sem, inc=1, device_id=peer_of(i, 0), device_id_type=MESH)
+    for copy in raw_loads:
+        copy.wait()
+    for i in (2, 1, 3):
+        yy = (y + i) % 4
+        sends.go(w_raw.at[yy], wy.at[y], h_s.at[i], h_r.at[y], device(z, yy, x, c))
     win_loads[1].wait()
     for i in (2, 1, 3):
         sends.go(wt.at[d], wt.at[d], t_s.at[i], t_r.at[d], device(z, y, (x + i) % 4, c))
@@ -196,9 +205,6 @@
         base[l] = total
 
     prepare(0)
-    pl.semaphore_wait(near_sem, 3)
-    for i in (2, 1, 3):
-        pl.semaphore_signal(far_sem, inc=1, device_id=peer_of(0, i), device_id_type=MESH)
     prepare(1)
 
     def read_out(l, raw, scale):
@@ -219,8 +225,7 @@
         for g in range(4):
             for h in range(2):
                 k = g * 2 + h
-                new_v[l, h * 16:h * 16 + 16, g, :] = ks[l, k] + push[k * 16:k * 16 + 16]
-        pltpu.make_async_copy(new_v.at[l], st_out.at[l], done.at[l]).start()
+                st_out[l, h * 16:h * 16 + 16, g, :] = ks[l, k] + push[k * 16:k * 16 + 16]
 
     for k in range(4):
         @pl.when(y != k)
@@ -233,22 +238,21 @@
     lane32 = lax.broadcasted_iota(jnp.int32, (32, 128), 1)
     for k in range(2):
         part_sq = jnp.where(row32 == lane32, square[k * 32:k * 32 + 32], 0.0)
-        sq[k] = jnp.broadcast_to(jnp.sum(part_sq, axis=0, keepdims=True), (8, 128))
-
-    pl.semaphore_wait(far_sem, 3)
-
-    def send_w0(k):
-        raw_loads[k].wait()
-        for i in (2, 1, 3, 0):
-            for j in range(2):
-                here = None
-                if i == 0:
-                    here = (z == x) & (y == 2 * c + j) & (y % 2 == c)
-                sends.go(w_raw.at[k, :, pl.ds(j * 256, 256)], w0.at[t, k],
-                         h_s.at[k, i * 2 + j], h_r.at[t, k],
-                         device(x, 2 * c + j, (x + i) % 4, y % 2), here)
-
-    send_w0(0)
+        sq[k] = jnp.sum(part_sq, axis=0, keepdims=True)
+
+    wy[y] = w_raw[y]
+    for k in range(4):
+        @pl.when(y != k)
+        def _(k=k):
+            arrived(wy.at[k], h_r.at[k])
+        turned = jnp.transpose(wy[k].reshape(128, 128).astype(F32)).astype(BF16)
+        for i in range(4):
+            wz[i, k] = turned[i * 32:i * 32 + 32]
+    for i in (2, 1, 3):
+        zz = (z + i) % 4
+        sends.go(wz.at[zz], w0.at[d, z], h_s.at[4 + i], h_r.at[4 + z], device(zz, y, x, c))
+    w0[d, z] = wz[z]
+
     for i in (0, 1, 3, 2):
         if i:
             arrived(wi.at[i], w_r.at[i])
@@ -262,16 +266,24 @@
             here = None if i else (x == z) & (c == k)
             sends.go(pb.at[i, k], bm.at[d], b_s.at[i * 2 + k], b_r.at[d], to, here)
             sends.go(sq.at[k], bq.at[d], q_s.at[i * 2 + k], q_r.at[d], to, here)
-    send_w0(1)
-    for j in range(2):
-        here = (z == x) & (y == 2 * c + j)
-        sends.go(xg.at[y, :, pl.ds(j * 256, 256)], res0.at[y % 2], e_s.at[0, j],
-                 e_r.at[0, y % 2], device(x, 2 * c + j, z, y // 2), here)
+    for i in range(4):
+        for k in range(2):
+            here = None if i else (x == z) & (c == k)
+            sends.go(xg.at[pl.ds(2 * k, 2), :, pl.ds(pl.multiple_of(y * 128, 128), 128)], res0.at[d],
+                     e_s.at[i * 2 + k], e_r.at[d], device((z - i) % 4, y, z, k), here)
     for i in range(4):
         k = ((x + i) % 4) * 2 + c
         if i:
             arrived(wt.at[k], t_r.at[k])
         sends.go(wt.at[k], wt.at[k], tf_s.at[i], t_r.at[k], device(z, y, x, other))
+
+    for k in range(4):
+        @pl.when(z != k)
+        def _(k=k):
+            arrived(w0.at[d, k], h_r.at[4 + k])
+    for i in (2, 1, 3):
+        sends.go(w0.at[d], w0.at[d], h_s.at[8 + i], hx_r.at[d], device(z, y, (x + i) % 4, c))
+    sends.go(w0.at[d], w0.at[d], hf_s.at[0], hx_r.at[d], device(z, y, x, other))
 
     for k in range(8):
         arrived(bq.at[k], q_r.at[k])
@@ -281,58 +293,76 @@
     for k in range(1, 8):
         squares = squares + bq[k]
         raw = raw + bm[k].astype(F32)
-    spread = jnp.broadcast_to(squares[0:1], (16, 128))
+    spread = jnp.broadcast_to(squares, (16, 128))
     first = jnp.sum(jnp.where(lane16 == row16, spread, 0.0), axis=1, keepdims=True)
     second = jnp.sum(jnp.where(lane16 == row16 + 16, spread, 0.0), axis=1, keepdims=True)
     scale = lax.rsqrt(jnp.where(low, first, second) * (1.0 / D) + EPS)
     side = y % 2
     ready = read_out(0, raw, scale)
-    rg[t] = jnp.where(side == 0, ready, pltpu.roll(ready, 64, 1)).astype(BF16)
+    rg[t] = ready.astype(BF16)
     for i, k in plane:
         sends.go(rg.at[t], rg.at[t], k_s.at[i * 4 + k], k_r.at[t], peer_of(i, k))
 
-    for k in range(2):
-        for i in range(8):
-            s = (i // 2) * 4 + (i % 2) * 2 + c
-            arrived(w0.at[s, k], h_r.at[s, k])
-            sends.go(w0.at[s, k], w0.at[s, k], hf_s.at[k, i], h_r.at[s, k],
-                     device(z, y, x, other))
     new_states(0, scale * raw)
-    for k in range(2):
-        for i in range(8):
-            s = (i // 2) * 4 + (i % 2) * 2 + other
-            arrived(w0.at[s, k], h_r.at[s, k])
-    for k in range(2):
-        arrived(res0.at[k], e_r.at[0, k])
+
+    lane = lax.broadcasted_iota(jnp.int32, (1, 128), 1) // 32
+
+    def regroup(tiles, first_block, mine):
+        out = None
+        for a, tile in enumerate(tiles):
+            piece = pltpu.roll(tile, 32 * ((mine(a) - first_block(a)) % 4), 1)
+            out = piece if out is None else jnp.where(lane == mine(a), piece, out)
+        return out
+
+    rest0 = jnp.concatenate(
+        [
+            regroup([waited(res0, e_r, 4 * g + a).reshape(32, 128).astype(F32) for a in range(4)],
+                    lambda a: z, lambda a: a)
+            for g in range(2)
+        ],
+        axis=1,
+    )
+    for i in range(4):
+        arrived(wt.at[2 * i + other], t_r.at[2 * i + other])
+    for k in range(8):
+        @pl.when(d != k)
+        def _(k=k):
+            arrived(gain_all.at[k], g_r.at[k])
+    for k in range(16):
+        tile = slice((k % 4) * 128, (k % 4) * 128 + 128)
+        for g in range(2):
+            wp[k, g] = regroup(
+                [wt[4 * g + a, :, tile].astype(F32) for a in range(4)], lambda a: k // 4, lambda a: a
+            ).astype(BF16)
+            gain_p[k, :, g * 128:g * 128 + 128] = regroup(
+                [gain_all[4 * g + a, :, tile] for a in range(4)], lambda a: k // 4, lambda a: a
+            )
+
+    for i in (1, 3, 2):
+        k = ((x + i) % 4) * 2 + c
+        arrived(w0.at[k], hx_r.at[k])
+        sends.go(w0.at[k], w0.at[k], hf_s.at[i], hx_r.at[k], device(z, y, x, other))
     for k in range(16):
         @pl.when(t != k)
         def _(k=k):
             arrived(rg.at[k], k_r.at[k])
     chunks = []
-    for k in range(0, 16, 2):
-        even, odd = rg[k], rg[k + 1]
-        top = jnp.where(low, even, odd)
-        bottom = jnp.where(low, odd, even)
-        bottom = jnp.concatenate([bottom[:, 64:], bottom[:, :64]], axis=1)
-        chunks.append(jnp.concatenate([top, bottom], axis=0))
-    left = jnp.concatenate(chunks, axis=1)
-    value = jnp.dot(left, w0[:, 0].reshape(1024, 256), preferred_element_type=F32)
-    gate = jnp.dot(left, w0[:, 1].reshape(1024, 256), preferred_element_type=F32)
-    current = res0[...].reshape(32, 256).astype(F32) + value * jax.nn.sigmoid(gate)
+    for k in range(16):
+        own = rg[k].astype(F32)
+        swapped = pltpu.roll(own, 64, 1)
+        chunks.append(jnp.concatenate(
+            [jnp.where(low, own, 0.0), jnp.where(low, swapped, 0.0),
+             jnp.where(low, 0.0, swapped), jnp.where(low, 0.0, own)], axis=0).astype(BF16))
+    for i in range(4):
+        arrived(w0.at[2 * i + other], hx_r.at[2 * i + other])
+    both = jnp.zeros((64, 256), F32)
+    for k in range(16):
+        both = both + nt(chunks[k], w0[:, k // 4, k % 4].reshape(256, 128))
+    current = rest0 + both[:32] * jax.nn.sigmoid(both[32:])
     xa[t] = current.astype(BF16)
     for i, k in plane:
         sends.go(xa.at[t], xa.at[t], n_s.at[i * 4 + k], n_r.at[t], peer_of(i, k))
-    for j in range(2):
-        here = (z == x) & (y == 2 * c + j)
-        sends.go(xa.at[t, pl.ds(j * 16, 16)], res1.at[y % 2], e_s.at[1, j],
-                 e_r.at[1, y % 2], device(x, 2 * c + j, z, y // 2), here)
-
-    for k in range(8):
-        @pl.when(d != k)
-        def _(k=k):
-            arrived(gain_all.at[k], g_r.at[k])
-    for i in range(4):
-        arrived(wt.at[2 * i + other], t_r.at[2 * i + other])
+
     for k in range(16):
         @pl.when(t != k)
         def _(k=k):
@@ -340,11 +370,10 @@
     total = jnp.zeros((32, 128), F32)
     square = jnp.zeros((32, 256), F32)
     for k in range(16):
-        half = slice((k % 2) * 256, (k % 2) * 256 + 256)
         wide = xa[k].astype(F32)
         square = square + wide * wide
-        gained = (wide * gain_all[k // 2, :, half]).astype(BF16)
-        w = wt[k // 2, :, half]
+        gained = (wide * gain_p[k]).astype(BF16)
+        w = jnp.concatenate([wp[k, 0], wp[k, 1]], axis=1)
         total = total + nt(gained, jnp.concatenate([w, w], axis=0))
     square = jnp.sum(square, axis=1, keepdims=True)
     raw = jnp.where(low, total[:16], total[16:])
@@ -363,12 +392,21 @@
                          c_r.at[x, y], device(z, yy, (x + i) % 4, (c + k) % 2), here)
     new_states(1, scale * raw)
 
+    half_to, d_to = z // 2, t % 8
+    for k in range(4):
+        tiles = []
+        for i in range(4):
+            piece = xa[i * 4 + k, pl.ds(pl.multiple_of(half_to * 16, 16), 16), :].astype(F32)
+            tiles.append(jnp.where(d_to // 4 == 0, piece[:, :128], piece[:, 128:]))
+        rest[:, k * 128:k * 128 + 128] = regroup(tiles, lambda a: d_to % 4, lambda a: a).astype(BF16)
+    here = (z == x) & (y == 2 * c + half_to) & (d == d_to)
+    sends.go(rest, res1, e_s.at[8], e_r.at[8],
+             device(x, 2 * c + half_to, d_to // 2, d_to % 2), here)
+
     for k in range(4):
         @pl.when(y != k)
         def _(k=k):
             arrived(wo.at[k], o_r.at[k])
-    for k in range(2):
-        arrived(res1.at[k], e_r.at[1, k])
     for i in range(4):
         for k in range(4):
             arrived(cr.at[i, k], c_r.at[i, k])
@@ -388,17 +426,13 @@
         arrived(rr.at[i], r_r.at[i])
         value = value + rr[i, 0].astype(F32)
         gate = gate + rr[i, 1].astype(F32)
-    before = jnp.concatenate([res1[0], res1[1]], axis=1).astype(F32)
-    out_v[...] = (before + value * jax.nn.sigmoid(gate)).astype(BF16)
-    copy = pltpu.make_async_copy(out_v, tok_out, done.at[L])
-    copy.start()
+    arrived(res1, e_r.at[8])
+    before = res1[...].astype(F32)
+    tok_out[...] = (before + value * jax.nn.sigmoid(gate)).astype(BF16)
     sends.finish()
-    copy.wait()
-    for l in range(L):
-        pltpu.make_async_copy(new_v.at[l], st_out.at[l], done.at[l]).wait()
-
-
-def body(*args):
+
+
+def layers(*args):
     args = list(args)
     args[2] = jnp.swapaxes(args[2], 1, 2)
     dma = pltpu.SemaphoreType.DMA
@@ -408,8 +442,12 @@
         v((4, 16, 512), BF16),
         v((4, 64, 512), BF16),
         v((8, 64, 512), BF16),
-        v((2, 64, 512), BF16),
-        v((16, 2, 64, 256), BF16),
+        v((4, 2, 64, 128), BF16),
+        v((4, 2, 64, 128), BF16),
+        v((4, 4, 32, 128), BF16),
+        v((8, 4, 4, 32, 128), BF16),
+        v((16, 2, 64, 128), BF16),
+        v((16, 1, 256), F32),
         v((4, 2, 64, 512), BF16),
         v((L, 512), F32),
         v((8, 1, 512), F32),
@@ -425,21 +463,20 @@
         v((L, 16, 128), F32),
         v((L, 8, 16, 128), F32),
         v((4, 2, 16, 128), BF16),
-        v((2, 8, 128), F32),
+        v((2, 1, 128), F32),
         v((8, 16, 128), BF16),
-        v((8, 8, 128), F32),
+        v((8, 1, 128), F32),
         v((16, 16, 128), BF16),
-        v((2, 16, 256), BF16),
+        v((8, 2, 16, 128), BF16),
+        v((16, 512), BF16),
         v((16, 32, 256), BF16),
-        v((2, 16, 256), BF16),
+        v((16, 512), BF16),
         v((2, 16, 128), BF16),
         v((4, 4, 16, 128), BF16),
         v((4, 2, 16, 512), F32),
         v((4, 2, 16, 512), BF16),
         v((4, 2, 16, 512), BF16),
-        v((L, 32, 4, 128), F32),
-        v((16, 512), BF16),
-        dma((7,)), dma((1,)), dma((2,)), dma((2, 2)), dma((1,)),
+        dma((7,)), dma((1,)), dma((2,)), dma((2, 2)), dma((1,)), dma((8,)),
         dma((4,)), dma((4,)),
         dma((4,)), dma((4,)),
         dma((4,)), dma((4,)),
@@ -449,26 +486,49 @@
         dma((4,)), dma((4,)),
         dma((4,)), dma((8,)), dma((4,)),
         dma((8,)), dma((8,)),
-        dma((2, 8)), dma((16, 2)), dma((2, 8)),
+        dma((12,)), dma((12,)), dma((8,)),
+        dma((8,)),
         dma((16,)), dma((16,)),
         dma((16,)), dma((16,)),
-        dma((2, 2)), dma((2, 2)),
-        pltpu.SemaphoreType.REGULAR,
-        pltpu.SemaphoreType.REGULAR,
-        dma((L + 1,)),
+        dma((9,)), dma((9,)),
     ]
     return pl.pallas_call(
         kernel,
         out_shape=(
-            jax.ShapeDtypeStruct((16, 512), BF16),
-            jax.ShapeDtypeStruct((L, 32, 4, 128), F32),
+            pltpu.VMEM((16, 512), BF16),
+            pltpu.VMEM((L, 32, 4, 128), F32),
         ),
         in_specs=[anywhere] * 12,
-        out_specs=(anywhere, anywhere),
+        out_specs=(pl.BlockSpec(memory_space=pltpu.VMEM),)*2,
         scratch_shapes=scratch,
         compiler_params=pltpu.CompilerParams(collective_id=0, has_side_effects=True),
         name="layers",
     )(*args)
+
+
+def tail(new_tokens, new_states, tokens_out, states_out, sem):
+    copies = [
+        pltpu.make_async_copy(new_states, states_out, sem.at[0]),
+        pltpu.make_async_copy(new_tokens, tokens_out, sem.at[1]),
+    ]
+    for copy in copies:
+        copy.start()
+    for copy in copies:
+        copy.wait()
+
+
+def body(*args):
+    vmem = pl.BlockSpec(memory_space=pltpu.VMEM)
+    anywhere = pl.BlockSpec(memory_space=pl.ANY)
+    results = [pltpu.with_memory_space_constraint(a, pltpu.VMEM) for a in layers(*args)]
+    return pl.pallas_call(
+        tail,
+        out_shape=tuple(jax.ShapeDtypeStruct(a.shape, a.dtype) for a in results),
+        in_specs=[vmem] * 2,
+        out_specs=(anywhere, anywhere),
+        scratch_shapes=[pltpu.SemaphoreType.DMA((2,))],
+        name="tail",
+    )(*results)
 
 
 def solution(mesh):

time: 51.1 us -> 45.9 us (0.90)
  local copies, waits for them, and re-layouts: 2.89 us -> 0 us
  Pallas kernels: 47.4 us -> 45.1 us
    unnamed x2 -> x0, local copies, waits for them, and re-layouts: 2.89 us -> none
    pallas_call x1 -> x2, Pallas kernels: 47.4 us -> 45.1 us  [the longest x1 44.4 us: layers(): pl.pallas_call(kernel, out_shape=(pltpu.VMEM((16, 512), BF16), pltpu.VMEM...]
where the time goes in v3:
time: 45.9 us; the launch traced here: 45.7 us
  Pallas kernels  45.1 us (98%)
  between operations  0.64 us (1%)
    pallas_call x1, Pallas kernels, layers(): pl.pallas_call(kernel, out_shape=(pltpu.VMEM((16, 512), BF16), pltpu.VMEM...  44.4 us

profile of v3, /device:TPU:1, one launch (start us, length us, event | category | flops | bytes accessed | tf_op | source)
XLA Modules:
  0.0 45.7 jit_solution(3419687167985812882)
XLA Ops:
  0.6 44.4 %layers.1 = (bf16[16,512]{1,0:T(8,128)(2,1)S(1)}, f32[2,32,4,128]{3,2,1,0:T(4,128)S(1)}) custom-call(bf16[16,512]{1,0:T(8,128)(2,1)} %tok.1, f32[2,512]{1,0:T(2,128)} %gain.1, bf16[2,64,512]{2,1,0:T(8,128)(2,1)} %bitcast.1, f32[2,4,64]{2,1,0:T(4,128)} %decay.1, f32[2,4,64]{2,1,0:T(4,128)} %freq.1, f32[2,4]{1,0:T(2,128)} %step.1, f32[2,4,16,128]{3,2,1,0:T(8,128)} %sin.1, ...), custom_call_target="tpu_custom_call" | custom-call | tf_op jit(solution)/shard_map/layers/pallas_call | solution.py:495
  45.0 0.7 %tail.1 = (bf16[16,512]{1,0:T(8,128)(2,1)}, f32[2,32,4,128]{3,2,1,0:T(4,128)}) custom-call(bf16[16,512]{1,0:T(8,128)(2,1)S(1)} %get-tuple-element.4.new_tokens, f32[2,32,4,128]{3,2,1,0:T(4,128)S(1)} %get-tuple-element.5.new_states), custom_call_target="tpu_custom_call" | custom-call | tf_op jit(solution)/shard_map/tail/pallas_call | solution.py:524

commit v4 on v3

--- a/solution.py
+++ b/solution.py
@@ -71,7 +71,7 @@
     tok, gain, win, decay, freq, step, sin, rdo, skip, wv, wg, st,
     tok_out, st_out,
     xg, wi, wt, w_raw, wy, wz, w0, wp, gain_p, wo, gain_v, gain_all, decay_v, freq_v, step_v, sin_v, rdo_v, skip_v, st_v,
-    big_b, m3, base, ks, pb, sq, bm, bq, rg, res0, rest, xa, res1, cs, cr, part, rs, rr,
+    big_b, m3, base, ks, pb, sq, bm, bq, rg, res0, rest, xa, rest0, res1, cs, cr, part, rs, rr,
     load, load_st, load_w, load_o, load_x, load_r, a_s, a_r, w_s, w_r, o_s, o_r,
     b_s, b_r, q_s, q_r, c_s, c_r, r_s, r_r, t_s, t_r, tf_s, g_s, g_r, h_s, h_r, hf_s, hx_r,
     k_s, k_r, n_s, n_r, e_s, e_r,
@@ -140,10 +140,12 @@
             if i + k:
                 sends.go(gain_all.at[d], gain_all.at[d], g_s.at[i * 2 + k], g_r.at[d],
                          device(z, y, (x + i) % 4, (c + k) % 2))
-    for copy in wo_loads:
-        copy.wait()
-    for i in (2, 1, 3):
-        sends.go(wo.at[y], wo.at[y], o_s.at[i], o_r.at[y], device(z, (y + i) % 4, x, c))
+
+    def send_wo(k):
+        wo_loads[k].wait()
+        for i in (2, 1, 3):
+            sends.go(wo.at[y, k], wo.at[y, k], o_s.at[k, i], o_r.at[k, y],
+                     device(z, (y + i) % 4, x, c))
 
     for copy in small_loads:
         copy.wait()
@@ -250,8 +252,10 @@
             wz[i, k] = turned[i * 32:i * 32 + 32]
     for i in (2, 1, 3):
         zz = (z + i) % 4
-        sends.go(wz.at[zz], w0.at[d, z], h_s.at[4 + i], h_r.at[4 + z], device(zz, y, x, c))
-    w0[d, z] = wz[z]
+        sends.go(wz.at[zz], w0.at[c, x, z], h_s.at[4 + i], h_r.at[4 + z], device(zz, y, x, c))
+    w0[c, x, z] = wz[z]
+    send_wo(0)
+    send_wo(1)
 
     for i in (0, 1, 3, 2):
         if i:
@@ -267,23 +271,23 @@
             sends.go(pb.at[i, k], bm.at[d], b_s.at[i * 2 + k], b_r.at[d], to, here)
             sends.go(sq.at[k], bq.at[d], q_s.at[i * 2 + k], q_r.at[d], to, here)
     for i in range(4):
+        k = ((x + i) % 4) * 2 + c
+        if i:
+            arrived(wt.at[k], t_r.at[k])
+        sends.go(wt.at[k], wt.at[k], tf_s.at[i], t_r.at[k], device(z, y, x, other))
+
+    for k in range(4):
+        @pl.when(z != k)
+        def _(k=k):
+            arrived(w0.at[c, x, k], h_r.at[4 + k])
+    for i in range(4):
         for k in range(2):
             here = None if i else (x == z) & (c == k)
             sends.go(xg.at[pl.ds(2 * k, 2), :, pl.ds(pl.multiple_of(y * 128, 128), 128)], res0.at[d],
                      e_s.at[i * 2 + k], e_r.at[d], device((z - i) % 4, y, z, k), here)
-    for i in range(4):
-        k = ((x + i) % 4) * 2 + c
-        if i:
-            arrived(wt.at[k], t_r.at[k])
-        sends.go(wt.at[k], wt.at[k], tf_s.at[i], t_r.at[k], device(z, y, x, other))
-
-    for k in range(4):
-        @pl.when(z != k)
-        def _(k=k):
-            arrived(w0.at[d, k], h_r.at[4 + k])
-    for i in (2, 1, 3):
-        sends.go(w0.at[d], w0.at[d], h_s.at[8 + i], hx_r.at[d], device(z, y, (x + i) % 4, c))
-    sends.go(w0.at[d], w0.at[d], hf_s.at[0], hx_r.at[d], device(z, y, x, other))
+    for i in (2, 1, 3):
+        sends.go(w0.at[c, x], w0.at[c, x], h_s.at[8 + i], hx_r.at[c, x], device(z, y, (x + i) % 4, c))
+    sends.go(w0.at[c, x], w0.at[c, x], hf_s.at[0], hx_r.at[c, x], device(z, y, x, other))
 
     for k in range(8):
         arrived(bq.at[k], q_r.at[k])
@@ -314,14 +318,6 @@
             out = piece if out is None else jnp.where(lane == mine(a), piece, out)
         return out
 
-    rest0 = jnp.concatenate(
-        [
-            regroup([waited(res0, e_r, 4 * g + a).reshape(32, 128).astype(F32) for a in range(4)],
-                    lambda a: z, lambda a: a)
-            for g in range(2)
-        ],
-        axis=1,
-    )
     for i in range(4):
         arrived(wt.at[2 * i + other], t_r.at[2 * i + other])
     for k in range(8):
@@ -332,16 +328,21 @@
         tile = slice((k % 4) * 128, (k % 4) * 128 + 128)
         for g in range(2):
             wp[k, g] = regroup(
-                [wt[4 * g + a, :, tile].astype(F32) for a in range(4)], lambda a: k // 4, lambda a: a
+                [wt[2 * a + g, :, tile].astype(F32) for a in range(4)], lambda a: k // 4, lambda a: a
             ).astype(BF16)
-            gain_p[k, :, g * 128:g * 128 + 128] = regroup(
-                [gain_all[4 * g + a, :, tile] for a in range(4)], lambda a: k // 4, lambda a: a
+            gain_p[k, g] = regroup(
+                [gain_all[2 * a + g, :, tile] for a in range(4)], lambda a: k // 4, lambda a: a
             )
 
     for i in (1, 3, 2):
-        k = ((x + i) % 4) * 2 + c
-        arrived(w0.at[k], hx_r.at[k])
-        sends.go(w0.at[k], w0.at[k], hf_s.at[i], hx_r.at[k], device(z, y, x, other))
+        k = (x + i) % 4
+        arrived(w0.at[c, k], hx_r.at[c, k])
+        sends.go(w0.at[c, k], w0.at[c, k], hf_s.at[i], hx_r.at[c, k], device(z, y, x, other))
+    for g in range(2):
+        rest0[g] = regroup(
+            [waited(res0, e_r, 2 * a + g).reshape(32, 128).astype(F32) for a in range(4)],
+            lambda a: z, lambda a: a,
+        )
     for k in range(16):
         @pl.when(t != k)
         def _(k=k):
@@ -353,28 +354,37 @@
         chunks.append(jnp.concatenate(
             [jnp.where(low, own, 0.0), jnp.where(low, swapped, 0.0),
              jnp.where(low, 0.0, swapped), jnp.where(low, 0.0, own)], axis=0).astype(BF16))
-    for i in range(4):
-        arrived(w0.at[2 * i + other], hx_r.at[2 * i + other])
-    both = jnp.zeros((64, 256), F32)
-    for k in range(16):
-        both = both + nt(chunks[k], w0[:, k // 4, k % 4].reshape(256, 128))
-    current = rest0 + both[:32] * jax.nn.sigmoid(both[32:])
-    xa[t] = current.astype(BF16)
-    for i, k in plane:
-        sends.go(xa.at[t], xa.at[t], n_s.at[i * 4 + k], n_r.at[t], peer_of(i, k))
-
-    for k in range(16):
-        @pl.when(t != k)
-        def _(k=k):
-            arrived(xa.at[k], n_r.at[k])
+    left = [jnp.concatenate(chunks[k:k + 2], axis=1) for k in range(0, 16, 2)]
+    for which in (c, other):
+        if which is other:
+            for i in range(4):
+                arrived(w0.at[other, i], hx_r.at[other, i])
+        both = jnp.zeros((64, 128), F32)
+        for j in range(8):
+            right = [w0[which, :, k // 4, k % 4].reshape(128, 128) for k in (2 * j, 2 * j + 1)]
+            both = both + nt(left[j], jnp.concatenate(right, axis=1))
+        xa[t, which] = (rest0[which] + both[:32] * jax.nn.sigmoid(both[32:])).astype(BF16)
+        for i, k in plane:
+            sends.go(xa.at[t, which], xa.at[t, which], n_s.at[which, i * 4 + k],
+                     n_r.at[which, t], peer_of(i, k))
+
     total = jnp.zeros((32, 128), F32)
-    square = jnp.zeros((32, 256), F32)
-    for k in range(16):
-        wide = xa[k].astype(F32)
-        square = square + wide * wide
-        gained = (wide * gain_p[k]).astype(BF16)
-        w = jnp.concatenate([wp[k, 0], wp[k, 1]], axis=1)
-        total = total + nt(gained, jnp.concatenate([w, w], axis=0))
+    square = jnp.zeros((32, 128), F32)
+    near_first = [(0, 0)] + plane[::-1]
+    for which in (c, other):
+        for j in range(0, 16, 2):
+            gained, right = [], []
+            for i, k in near_first[j:j + 2]:
+                s = ((z + i) % 4) * 4 + (y + k) % 4
+                if i + k:
+                    arrived(xa.at[s, which], n_r.at[which, s])
+                wide = xa[s, which].astype(F32)
+                square = square + wide * wide
+                gained.append((wide * gain_p[s, which]).astype(BF16))
+                right.append(wp[s, which])
+            right = jnp.concatenate(right, axis=1)
+            right = jnp.concatenate([right, right], axis=0)
+            total = total + nt(jnp.concatenate(gained, axis=1), right)
     square = jnp.sum(square, axis=1, keepdims=True)
     raw = jnp.where(low, total[:16], total[16:])
     scale = lax.rsqrt(jnp.where(low, square[:16], square[16:]) * (1.0 / D) + EPS)
@@ -396,9 +406,10 @@
     for k in range(4):
         tiles = []
         for i in range(4):
-            piece = xa[i * 4 + k, pl.ds(pl.multiple_of(half_to * 16, 16), 16), :].astype(F32)
-            tiles.append(jnp.where(d_to // 4 == 0, piece[:, :128], piece[:, 128:]))
-        rest[:, k * 128:k * 128 + 128] = regroup(tiles, lambda a: d_to % 4, lambda a: a).astype(BF16)
+            tiles.append(
+                xa[i * 4 + k, d_to % 2, pl.ds(pl.multiple_of(half_to * 16, 16), 16), :].astype(F32)
+            )
+        rest[:, k * 128:k * 128 + 128] = regroup(tiles, lambda a: d_to // 2, lambda a: a).astype(BF16)
     here = (z == x) & (y == 2 * c + half_to) & (d == d_to)
     sends.go(rest, res1, e_s.at[8], e_r.at[8],
              device(x, 2 * c + half_to, d_to // 2, d_to % 2), here)
@@ -406,7 +417,8 @@
     for k in range(4):
         @pl.when(y != k)
         def _(k=k):
-            arrived(wo.at[k], o_r.at[k])
+            for i in range(2):
+                arrived(wo.at[k, i], o_r.at[i, k])
     for i in range(4):
         for k in range(4):
             arrived(cr.at[i, k], c_r.at[i, k])
@@ -445,9 +457,9 @@
         v((4, 2, 64, 128), BF16),
         v((4, 2, 64, 128), BF16),
         v((4, 4, 32, 128), BF16),
-        v((8, 4, 4, 32, 128), BF16),
+        v((2, 4, 4, 4, 32, 128), BF16),
         v((16, 2, 64, 128), BF16),
-        v((16, 1, 256), F32),
+        v((16, 2, 1, 128), F32),
         v((4, 2, 64, 512), BF16),
         v((L, 512), F32),
         v((8, 1, 512), F32),
@@ -469,7 +481,8 @@
         v((16, 16, 128), BF16),
         v((8, 2, 16, 128), BF16),
         v((16, 512), BF16),
-        v((16, 32, 256), BF16),
+        v((16, 2, 32, 128), BF16),
+        v((2, 32, 128), F32),
         v((16, 512), BF16),
         v((2, 16, 128), BF16),
         v((4, 4, 16, 128), BF16),
@@ -479,7 +492,7 @@
         dma((7,)), dma((1,)), dma((2,)), dma((2, 2)), dma((1,)), dma((8,)),
         dma((4,)), dma((4,)),
         dma((4,)), dma((4,)),
-        dma((4,)), dma((4,)),
+        dma((2, 4)), dma((2, 4)),
         dma((8,)), dma((8,)),
         dma((8,)), dma((8,)),
         dma((16,)), dma((4, 4)),
@@ -487,9 +500,9 @@
         dma((4,)), dma((8,)), dma((4,)),
         dma((8,)), dma((8,)),
         dma((12,)), dma((12,)), dma((8,)),
-        dma((8,)),
+        dma((2, 4)),
         dma((16,)), dma((16,)),
-        dma((16,)), dma((16,)),
+        dma((2, 16)), dma((2, 16)),
         dma((9,)), dma((9,)),
     ]
     return pl.pallas_call(

time: 45.9 us -> 44.4 us (0.967)
  Pallas kernels: 45.1 us -> 43.6 us
    pallas_call x1, Pallas kernels: 44.4 us -> 43 us  [layers(): pl.pallas_call(kernel, out_shape=(pltpu.VMEM((16, 512), BF16), pltpu.VMEM...]
where the time goes in v4:
time: 44.4 us; the launch traced here: 44.3 us
  Pallas kernels  43.6 us (98%)
  between operations  0.64 us (1%)
    pallas_call x1, Pallas kernels, layers(): pl.pallas_call(kernel, out_shape=(pltpu.VMEM((16, 512), BF16), pltpu.VMEM...  43 us

profile of v4, /device:TPU:1, one launch (start us, length us, event | category | flops | bytes accessed | tf_op | source)
XLA Modules:
  0.0 44.3 jit_solution(6317745339132405674)
XLA Ops:
  0.6 43.0 %layers.1 = (bf16[16,512]{1,0:T(8,128)(2,1)S(1)}, f32[2,32,4,128]{3,2,1,0:T(4,128)S(1)}) custom-call(bf16[16,512]{1,0:T(8,128)(2,1)} %tok.1, f32[2,512]{1,0:T(2,128)} %gain.1, bf16[2,64,512]{2,1,0:T(8,128)(2,1)} %bitcast.1, f32[2,4,64]{2,1,0:T(4,128)} %decay.1, f32[2,4,64]{2,1,0:T(4,128)} %freq.1, f32[2,4]{1,0:T(2,128)} %step.1, f32[2,4,16,128]{3,2,1,0:T(8,128)} %sin.1, ...), custom_call_target="tpu_custom_call" | custom-call | tf_op jit(solution)/shard_map/layers/pallas_call | solution.py:508
  43.6 0.7 %tail.1 = (bf16[16,512]{1,0:T(8,128)(2,1)}, f32[2,32,4,128]{3,2,1,0:T(4,128)}) custom-call(bf16[16,512]{1,0:T(8,128)(2,1)S(1)} %get-tuple-element.4.new_tokens, f32[2,32,4,128]{3,2,1,0:T(4,128)S(1)} %get-tuple-element.5.new_states), custom_call_target="tpu_custom_call" | custom-call | tf_op jit(solution)/shard_map/tail/pallas_call | solution.py:537

commit v5 on v4

--- a/solution.py
+++ b/solution.py
@@ -48,8 +48,10 @@
 
         self.waits.append((jnp.logical_not(here), copy))
 
-    def finish(self):
-        for away, copy in self.waits:
+    def finish(self, but=0):
+        last = len(self.waits) - but
+        done, self.waits = self.waits[:last], self.waits[last:]
+        for away, copy in done:
             if away is None:
                 copy.wait_send()
             else:
@@ -71,7 +73,7 @@
     tok, gain, win, decay, freq, step, sin, rdo, skip, wv, wg, st,
     tok_out, st_out,
     xg, wi, wt, w_raw, wy, wz, w0, wp, gain_p, wo, gain_v, gain_all, decay_v, freq_v, step_v, sin_v, rdo_v, skip_v, st_v,
-    big_b, m3, base, ks, pb, sq, bm, bq, rg, res0, rest, xa, rest0, res1, cs, cr, part, rs, rr,
+    big_b, m3, base, ks, pb, sq, bm, bq, rg, pt, res0, xs, rest, xa, rest0, res1, cs, cr, part, rs, rr,
     load, load_st, load_w, load_o, load_x, load_r, a_s, a_r, w_s, w_r, o_s, o_r,
     b_s, b_r, q_s, q_r, c_s, c_r, r_s, r_r, t_s, t_r, tf_s, g_s, g_r, h_s, h_r, hf_s, hx_r,
     k_s, k_r, n_s, n_r, e_s, e_r,
@@ -113,8 +115,8 @@
     plane = [(i, k) for i in range(4) for k in range(4) if i + k]
     plane.sort(key=lambda ik: -(min(ik[0], 4 - ik[0]) + min(ik[1], 4 - ik[1])))
 
-    def peer_of(i, k):
-        return device((z + i) % 4, (y + k) % 4, x, c)
+    def peer_of(i, k, core):
+        return device((z + i) % 4, (y + k) % 4, x, core)
 
     sends = Sends()
     win_loads[0].wait()
@@ -229,6 +231,15 @@
                 k = g * 2 + h
                 st_out[l, h * 16:h * 16 + 16, g, :] = ks[l, k] + push[k * 16:k * 16 + 16]
 
+    lane = lax.broadcasted_iota(jnp.int32, (1, 128), 1) // 32
+
+    def regroup(tiles, first_block, mine):
+        out = None
+        for a, tile in enumerate(tiles):
+            piece = pltpu.roll(tile, 32 * ((mine(a) - first_block(a)) % 4), 1)
+            out = piece if out is None else jnp.where(lane == mine(a), piece, out)
+        return out
+
     for k in range(4):
         @pl.when(y != k)
         def _(k=k):
@@ -242,22 +253,7 @@
         part_sq = jnp.where(row32 == lane32, square[k * 32:k * 32 + 32], 0.0)
         sq[k] = jnp.sum(part_sq, axis=0, keepdims=True)
 
-    wy[y] = w_raw[y]
-    for k in range(4):
-        @pl.when(y != k)
-        def _(k=k):
-            arrived(wy.at[k], h_r.at[k])
-        turned = jnp.transpose(wy[k].reshape(128, 128).astype(F32)).astype(BF16)
-        for i in range(4):
-            wz[i, k] = turned[i * 32:i * 32 + 32]
-    for i in (2, 1, 3):
-        zz = (z + i) % 4
-        sends.go(wz.at[zz], w0.at[c, x, z], h_s.at[4 + i], h_r.at[4 + z], device(zz, y, x, c))
-    w0[c, x, z] = wz[z]
-    send_wo(0)
-    send_wo(1)
-
-    for i in (0, 1, 3, 2):
+    def project(i):
         if i:
             arrived(wi.at[i], w_r.at[i])
         prod = nt(gained, jnp.concatenate([wi[i], wi[i]], axis=0))
@@ -270,24 +266,50 @@
             here = None if i else (x == z) & (c == k)
             sends.go(pb.at[i, k], bm.at[d], b_s.at[i * 2 + k], b_r.at[d], to, here)
             sends.go(sq.at[k], bq.at[d], q_s.at[i * 2 + k], q_r.at[d], to, here)
+
+    project(0)
+
+    wy[y] = w_raw[y]
+    for k in range(4):
+        @pl.when(y != k)
+        def _(k=k):
+            arrived(wy.at[k], h_r.at[k])
+        turned = jnp.transpose(wy[k].reshape(128, 128).astype(F32)).astype(BF16)
+        for i in range(4):
+            wz[i, k] = turned[i * 32:i * 32 + 32]
+    for i in (2, 1, 3):
+        zz = (z + i) % 4
+        sends.go(wz.at[zz], w0.at[x, z], h_s.at[4 + i], h_r.at[4 + z], device(zz, y, x, c))
+    w0[x, z] = wz[z]
+
+    def replicate(i):
+        zz = (z + i) % 4
+        if i:
+            arrived(w0.at[x, zz], h_r.at[4 + zz])
+        for k in (2, 1, 3):
+            sends.go(w0.at[x, zz], w0.at[x, zz], hf_s.at[i, k], hx_r.at[x, zz],
+                     device(z, y, (x + k) % 4, c))
+
+    send_wo(0)
+    send_wo(1)
+
+    for i in (1, 3, 2):
+        project(i)
     for i in range(4):
         k = ((x + i) % 4) * 2 + c
         if i:
             arrived(wt.at[k], t_r.at[k])
         sends.go(wt.at[k], wt.at[k], tf_s.at[i], t_r.at[k], device(z, y, x, other))
 
-    for k in range(4):
-        @pl.when(z != k)
-        def _(k=k):
-            arrived(w0.at[c, x, k], h_r.at[4 + k])
+    for i in (0, 1, 3, 2):
+        replicate(i)
+    mine = pl.ds(pl.multiple_of(y * 128, 128), 128)
+    blocks = [xg[a, :, mine].astype(F32) for a in range(4)]
     for i in range(4):
-        for k in range(2):
-            here = None if i else (x == z) & (c == k)
-            sends.go(xg.at[pl.ds(2 * k, 2), :, pl.ds(pl.multiple_of(y * 128, 128), 128)], res0.at[d],
-                     e_s.at[i * 2 + k], e_r.at[d], device((z - i) % 4, y, z, k), here)
-    for i in (2, 1, 3):
-        sends.go(w0.at[c, x], w0.at[c, x], h_s.at[8 + i], hx_r.at[c, x], device(z, y, (x + i) % 4, c))
-    sends.go(w0.at[c, x], w0.at[c, x], hf_s.at[0], hx_r.at[c, x], device(z, y, x, other))
+        zz = (z - i) % 4
+        pt[i] = regroup(blocks, lambda a: zz, lambda a: a).astype(BF16)
+        here = None if i else x == z
+        sends.go(pt.at[i], res0.at[x], e_s.at[i], e_r.at[x], device(zz, y, z, c), here)
 
     for k in range(8):
         arrived(bq.at[k], q_r.at[k])
@@ -303,20 +325,14 @@
     scale = lax.rsqrt(jnp.where(low, first, second) * (1.0 / D) + EPS)
     side = y % 2
     ready = read_out(0, raw, scale)
-    rg[t] = ready.astype(BF16)
-    for i, k in plane:
-        sends.go(rg.at[t], rg.at[t], k_s.at[i * 4 + k], k_r.at[t], peer_of(i, k))
+    rg[c, t] = ready.astype(BF16)
+    for i, k in plane + [(0, 0)]:
+        for n, core in enumerate((c, other)):
+            if i + k + n:
+                sends.go(rg.at[c, t], rg.at[c, t], k_s.at[n, i * 4 + k], k_r.at[c, t],
+                         peer_of(i, k, core))
 
     new_states(0, scale * raw)
-
-    lane = lax.broadcasted_iota(jnp.int32, (1, 128), 1) // 32
-
-    def regroup(tiles, first_block, mine):
-        out = None
-        for a, tile in enumerate(tiles):
-            piece = pltpu.roll(tile, 32 * ((mine(a) - first_block(a)) % 4), 1)
-            out = piece if out is None else jnp.where(lane == mine(a), piece, out)
-        return out
 
     for i in range(4):
         arrived(wt.at[2 * i + other], t_r.at[2 * i + other])
@@ -334,57 +350,61 @@
                 [gain_all[2 * a + g, :, tile] for a in range(4)], lambda a: k // 4, lambda a: a
             )
 
-    for i in (1, 3, 2):
-        k = (x + i) % 4
-        arrived(w0.at[c, k], hx_r.at[c, k])
-        sends.go(w0.at[c, k], w0.at[c, k], hf_s.at[i], hx_r.at[c, k], device(z, y, x, other))
-    for g in range(2):
-        rest0[g] = regroup(
-            [waited(res0, e_r, 2 * a + g).reshape(32, 128).astype(F32) for a in range(4)],
-            lambda a: z, lambda a: a,
+    for a in range(4):
+        arrived(res0.at[a], e_r.at[a])
+    for k in range(4):
+        rest0[k] = regroup(
+            [res0[a].astype(F32) for a in range(4)], lambda a: k, lambda a: a
         )
-    for k in range(16):
-        @pl.when(t != k)
-        def _(k=k):
-            arrived(rg.at[k], k_r.at[k])
+
+    near_first = [(0, 0)] + plane[::-1]
+    for i, k in near_first:
+        s = ((z + i) % 4) * 4 + (y + k) % 4
+        for n, core in enumerate((c, other)):
+            if i + k + n:
+                arrived(rg.at[core, s], k_r.at[core, s])
     chunks = []
     for k in range(16):
-        own = rg[k].astype(F32)
-        swapped = pltpu.roll(own, 64, 1)
-        chunks.append(jnp.concatenate(
-            [jnp.where(low, own, 0.0), jnp.where(low, swapped, 0.0),
-             jnp.where(low, 0.0, swapped), jnp.where(low, 0.0, own)], axis=0).astype(BF16))
-    left = [jnp.concatenate(chunks[k:k + 2], axis=1) for k in range(0, 16, 2)]
-    for which in (c, other):
-        if which is other:
-            for i in range(4):
-                arrived(w0.at[other, i], hx_r.at[other, i])
-        both = jnp.zeros((64, 128), F32)
-        for j in range(8):
-            right = [w0[which, :, k // 4, k % 4].reshape(128, 128) for k in (2 * j, 2 * j + 1)]
-            both = both + nt(left[j], jnp.concatenate(right, axis=1))
-        xa[t, which] = (rest0[which] + both[:32] * jax.nn.sigmoid(both[32:])).astype(BF16)
-        for i, k in plane:
-            sends.go(xa.at[t, which], xa.at[t, which], n_s.at[which, i * 4 + k],
-                     n_r.at[which, t], peer_of(i, k))
+        tops, bottoms = [], []
+        for n in range(2):
+            own = rg[n, k].astype(F32)
+            swapped = pltpu.roll(own, 64, 1)
+            tops += [jnp.where(low, own, 0.0), jnp.where(low, swapped, 0.0)]
+            bottoms += [jnp.where(low, 0.0, swapped), jnp.where(low, 0.0, own)]
+        chunks.append(jnp.concatenate(tops + bottoms, axis=0).astype(BF16))
+    for i in (1, 3, 2):
+        for k in range(4):
+            arrived(w0.at[(x + i) % 4, k], hx_r.at[(x + i) % 4, k])
+    both = jnp.zeros((128, 128), F32)
+    for j in range(0, 16, 2):
+        right = [w0[:, k // 4, k % 4].reshape(128, 128) for k in (j, j + 1)]
+        left = jnp.concatenate(chunks[j:j + 2], axis=1)
+        both = both + nt(left, jnp.concatenate(right, axis=1))
+    current = rest0[...].reshape(64, 128) + both[:64] * jax.nn.sigmoid(both[64:])
+    xs[0] = current[:32].astype(BF16)
+    xs[1] = current[32:].astype(BF16)
+    for i, k in plane + [(0, 0)]:
+        for n, core in enumerate((c, other)):
+            if i + k + n:
+                sends.go(xs.at[core], xa.at[t, c], n_s.at[n, i * 4 + k], n_r.at[c, t],
+                         peer_of(i, k, core))
+    xa[t, c] = xs[c]
 
     total = jnp.zeros((32, 128), F32)
     square = jnp.zeros((32, 128), F32)
-    near_first = [(0, 0)] + plane[::-1]
-    for which in (c, other):
-        for j in range(0, 16, 2):
-            gained, right = [], []
-            for i, k in near_first[j:j + 2]:
-                s = ((z + i) % 4) * 4 + (y + k) % 4
-                if i + k:
-                    arrived(xa.at[s, which], n_r.at[which, s])
-                wide = xa[s, which].astype(F32)
-                square = square + wide * wide
-                gained.append((wide * gain_p[s, which]).astype(BF16))
-                right.append(wp[s, which])
-            right = jnp.concatenate(right, axis=1)
-            right = jnp.concatenate([right, right], axis=0)
-            total = total + nt(jnp.concatenate(gained, axis=1), right)
+    for i, k in near_first:
+        s = ((z + i) % 4) * 4 + (y + k) % 4
+        for n, core in enumerate((c, other)):
+            if i + k + n:
+                arrived(xa.at[s, core], n_r.at[core, s])
+        gained = []
+        for n in range(2):
+            wide = xa[s, n].astype(F32)
+            square = square + wide * wide
+            gained.append((wide * gain_p[s, n]).astype(BF16))
+        right = jnp.concatenate([wp[s, 0], wp[s, 1]], axis=1)
+        right = jnp.concatenate([right, right], axis=0)
+        total = total + nt(jnp.concatenate(gained, axis=1), right)
     square = jnp.sum(square, axis=1, keepdims=True)
     raw = jnp.where(low, total[:16], total[16:])
     scale = lax.rsqrt(jnp.where(low, square[:16], square[16:]) * (1.0 / D) + EPS)
@@ -430,12 +450,14 @@
         for i in range(4):
             part[i, k] = prod[i * 16:i * 16 + 16]
             rs[i, k] = prod[i * 16:i * 16 + 16].astype(BF16)
-    for i in (2, 1, 3):
-        zz = (z + i) % 4
-        sends.go(rs.at[zz], rr.at[i], r_s.at[i], r_r.at[i], device(zz, y, x, c))
+        for i in (2, 1, 3):
+            zz = (z + i) % 4
+            sends.go(rs.at[zz, k], rr.at[i, k], r_s.at[k, i], r_r.at[k, i], device(zz, y, x, c))
+    sends.finish(6)
     value, gate = part[z, 0], part[z, 1]
     for i in (1, 3, 2):
-        arrived(rr.at[i], r_r.at[i])
+        for k in range(2):
+            arrived(rr.at[i, k], r_r.at[k, i])
         value = value + rr[i, 0].astype(F32)
         gate = gate + rr[i, 1].astype(F32)
     arrived(res1, e_r.at[8])
@@ -457,7 +479,7 @@
         v((4, 2, 64, 128), BF16),
         v((4, 2, 64, 128), BF16),
         v((4, 4, 32, 128), BF16),
-        v((2, 4, 4, 4, 32, 128), BF16),
+        v((4, 4, 4, 32, 128), BF16),
         v((16, 2, 64, 128), BF16),
         v((16, 2, 1, 128), F32),
         v((4, 2, 64, 512), BF16),
@@ -478,11 +500,13 @@
         v((2, 1, 128), F32),
         v((8, 16, 128), BF16),
         v((8, 1, 128), F32),
-        v((16, 16, 128), BF16),
-        v((8, 2, 16, 128), BF16),
+        v((2, 16, 16, 128), BF16),
+        v((4, 16, 128), BF16),
+        v((4, 16, 128), BF16),
+        v((2, 32, 128), BF16),
         v((16, 512), BF16),
         v((16, 2, 32, 128), BF16),
-        v((2, 32, 128), F32),
+        v((4, 16, 128), F32),
         v((16, 512), BF16),
         v((2, 16, 128), BF16),
         v((4, 4, 16, 128), BF16),
@@ -496,12 +520,12 @@
         dma((8,)), dma((8,)),
         dma((8,)), dma((8,)),
         dma((16,)), dma((4, 4)),
-        dma((4,)), dma((4,)),
+        dma((2, 4)), dma((2, 4)),
         dma((4,)), dma((8,)), dma((4,)),
         dma((8,)), dma((8,)),
-        dma((12,)), dma((12,)), dma((8,)),
-        dma((2, 4)),
-        dma((16,)), dma((16,)),
+        dma((8,)), dma((8,)), dma((4, 4)),
+        dma((4, 4)),
+        dma((2, 16)), dma((2, 16)),
         dma((2, 16)), dma((2, 16)),
         dma((9,)), dma((9,)),
     ]

time: 44.4 us -> 42.7 us (0.962)
  Pallas kernels: 43.6 us -> 41.9 us
    pallas_call x1, Pallas kernels: 43 us -> 41.2 us  [layers(): pl.pallas_call(kernel, out_shape=(pltpu.VMEM((16, 512), BF16), pltpu.VMEM...]
where the time goes in v5:
time: 42.7 us; the launch traced here: 42.6 us
  Pallas kernels  41.9 us (98%)
  between operations  0.64 us (1%)
    pallas_call x1, Pallas kernels, layers(): pl.pallas_call(kernel, out_shape=(pltpu.VMEM((16, 512), BF16), pltpu.VMEM...  41.2 us

profile of v5, /device:TPU:1, one launch (start us, length us, event | category | flops | bytes accessed | tf_op | source)
XLA Modules:
  0.0 42.6 jit_solution(18098983429731782258)
XLA Ops:
  0.6 41.2 %layers.1 = (bf16[16,512]{1,0:T(8,128)(2,1)S(1)}, f32[2,32,4,128]{3,2,1,0:T(4,128)S(1)}) custom-call(bf16[16,512]{1,0:T(8,128)(2,1)} %tok.1, f32[2,512]{1,0:T(2,128)} %gain.1, bf16[2,64,512]{2,1,0:T(8,128)(2,1)} %bitcast.1, f32[2,4,64]{2,1,0:T(4,128)} %decay.1, f32[2,4,64]{2,1,0:T(4,128)} %freq.1, f32[2,4]{1,0:T(2,128)} %step.1, f32[2,4,16,128]{3,2,1,0:T(8,128)} %sin.1, ...), custom_call_target="tpu_custom_call" | custom-call | tf_op jit(solution)/shard_map/layers/pallas_call | solution.py:532
  41.9 0.7 %tail.1 = (bf16[16,512]{1,0:T(8,128)(2,1)}, f32[2,32,4,128]{3,2,1,0:T(4,128)}) custom-call(bf16[16,512]{1,0:T(8,128)(2,1)S(1)} %get-tuple-element.4.new_tokens, f32[2,32,4,128]{3,2,1,0:T(4,128)S(1)} %get-tuple-element.5.new_states), custom_call_target="tpu_custom_call" | custom-call | tf_op jit(solution)/shard_map/tail/pallas_call | solution.py:561
